TPU v7x, 256 devices: a 8x8x2 block of a 8x8x16 slice. The times are simulated.
256 devices in a mesh: grp: 2 (over z), sp: 16 (over y, core), tp: 8 (over x).
Axes of the slice: x: 8, y: 8, z: 2, core: 2. Of those that a mesh axis runs over, the one named last changes fastest.
The devices are a block of a 8x8x16 slice.
Arguments:
- stream: bfloat16 [8192, 2048], P(('grp', 'sp'), 'tp'), parts along dimension 0, may hold values from -6 to 6
- documents: int32 [8192], P(('grp', 'sp')), parts along dimension 0, may hold values from 0 to 7, never falling along the last dimension, each value on 1 to 768 neighbouring positions
- q_weight: bfloat16 [2, 2048, 2048], P(None, 'sp', 'tp'), may hold values from -0.125 to 0.125
- k_weight: bfloat16 [2, 2048, 2048], P(None, 'sp', 'tp'), may hold values from -0.125 to 0.125
- v_weight: bfloat16 [2, 2048, 2048], P(None, 'sp', 'tp'), may hold values from -0.125 to 0.125
- out_weight: bfloat16 [2, 2048, 2048], P(None, 'sp', 'tp'), may hold values from -0.125 to 0.125
- pre_gain: float32 [2, 2048], replicated, may hold values from 0.1 to 1.9
- post_gain: float32 [2, 2048], P(None, 'tp'), may hold values from 0.1 to 1.9
- offset_bias: float32 [2, 32, 15, 31], P(None, 'tp'), may hold values from -3 to 263
Outputs:
- result_stream: bfloat16 [8192, 2048], P(('grp', 'sp'), 'tp'), parts along dimension 0
There are 2 independent parts, one for each index of `grp`. A program takes and returns all parts, laid end to end along the dimension named above; an argument that names none is the same for every part. Nothing has to cross between parts.
All inputs are finite; a program needn't handle non-finite values.
Results may differ from a plain program's by a relative error of at most 0.02.
Values may be sent and summed in bfloat16 or wider, within the bound.
No kernel may reach another device: no remote copies, remote signals or barrier semaphores. Data moves between devices by JAX's collectives and lax.ppermute only.
A program may use at most 128 MiB of HBM per device.

v0:
```python
import functools

import jax
import jax.numpy as jnp
from jax import lax
from jax.experimental import pallas as pl
from jax.experimental.pallas import tpu as pltpu
from jax.sharding import PartitionSpec as P


HEAD_DIM = 64
D = 2048
GRID_W = 64
NA_ROWS = 8
NA_COLS = 16
HALF_ROWS = NA_ROWS // 2
LANES = 128
PAD_ROWS = 8
MASKED = -1e30

EPS = 1e-06


VMEM = pl.BlockSpec(memory_space=pltpu.VMEM)


def copies_for(x, axis):
    return jnp.broadcast_to(x, (lax.axis_size(axis), *x.shape))


def exchange(x, axis):
    return lax.all_to_all(x, axis, split_axis=0, concat_axis=0, tiled=True)


def partner(x):
    count = lax.axis_size("sp")
    return lax.ppermute(x, "sp", [(i, i ^ 1) for i in range(count)])


def across(x):
    count = lax.axis_size("sp")
    moves = [(i, i + 1) for i in range(1, count - 1, 2)]
    return lax.ppermute(x, "sp", moves + [(j, i) for i, j in moves])


def ring(chunk):
    count = lax.axis_size("sp")
    half = count // 2
    up = [(i, (i + 2) % count) for i in range(count)]
    down = [(j, i) for i, j in up]
    slots = {0: chunk}
    left = right = chunk
    for k in range(1, half // 2 + 1):
        left = lax.ppermute(left, "sp", up)
        slots[-k] = left
        if k < half - half // 2:
            right = lax.ppermute(right, "sp", down)
            slots[k] = right
    return slots


def stack_kernel(*refs):
    *in_refs, out_ref = refs
    for n, ref in enumerate(in_refs):
        out_ref[n] = ref[...]


def stacked(arrays):
    rows, width = arrays[0].shape
    return pl.pallas_call(
        stack_kernel,
        out_shape=jax.ShapeDtypeStruct((len(arrays), rows, width), arrays[0].dtype),
        in_specs=[VMEM] * len(arrays),
        out_specs=VMEM,
        name="stack",
        compiler_params=pltpu.CompilerParams(vmem_limit_bytes=8 * 2**20),
        cost_estimate=pl.CostEstimate(
            flops=len(arrays) * rows * width,
            bytes_accessed=4 * len(arrays) * rows * width,
            transcendentals=0,
        ),
    )(*arrays)


def with_partner(slots):
    weights = []
    for low, high in ((0, 2), (3, 3), (4, 4)):
        keys = tuple(k for k in sorted(slots, key=abs) if low <= abs(k) <= high)
        own = [slots[k] for k in keys]
        own = stacked(own) if len(own) > 1 else own[0][None]
        weights += [(keys, 0, own), (keys, 1, partner(own))]
    return weights


def weight_rows(weights):
    return sum(w.shape[0] * w.shape[1] for _, _, w in weights)


def weight_places(weights):
    return [(keys, other) for keys, other, _ in weights]


def place_weights(places, refs, w_all, first=0):
    me = lax.axis_index("sp")
    pairs = lax.axis_size("sp") // 2
    place, parity = me // 2, lax.rem(me, 2)
    width = w_all.shape[1]
    for (keys, other), ref in zip(places, refs):
        rows = ref.shape[1]
        for n, k in enumerate(keys):
            block = lax.rem(place + k + pairs, pairs) * 2
            block += 1 - parity if other else parity
            start = pl.multiple_of(block * rows, rows)
            w_all[pl.ds(start, rows), :] = ref[n, :, first : first + width]


def prepare_kernel(total_rows, doc_ref, near_ref, far_ref, table_ref, *out_refs):
    tokens = doc_ref.shape[1]
    rows_dev = tokens // GRID_W
    me = lax.axis_index("sp")
    first_row = me * rows_dev
    odd = jnp.full((1, tokens), lax.rem(me, 2), jnp.int32) == 1
    near, own, far = near_ref[...], doc_ref[...], far_ref[...]
    sides = (jnp.where(odd, near, far), own, jnp.where(odd, far, near))
    sides = [side.astype(jnp.float32) for side in sides]
    shape = (GRID_W, LANES)
    col = lax.broadcasted_iota(jnp.int32, shape, 0)
    lane = lax.broadcasted_iota(jnp.int32, shape, 1)
    upper = lane // GRID_W
    key_col = lane - upper * GRID_W
    col_first = jnp.clip(col - NA_COLS // 2, 0, GRID_W - NA_COLS)
    col_fits = (key_col >= col_first) & (key_col < col_first + NA_COLS)
    tiles_side = tokens // LANES
    columns = [
        jnp.broadcast_to(sides[1][:, t * LANES : (t + 1) * LANES], (LANES, LANES)).T
        for t in range(tiles_side)
    ]
    masks = {}
    for i in range(rows_dev):
        row_first = jnp.clip(first_row + i - HALF_ROWS, 0, total_rows - NA_ROWS)
        part = i * GRID_W % LANES
        doc_col = columns[i * GRID_W // LANES][part : part + GRID_W, :]
        for k in range(3 * tiles_side):
            key_row = first_row - HALF_ROWS + 2 * k + upper
            t = k % tiles_side
            doc_row = sides[k // tiles_side][:, t * LANES : (t + 1) * LANES]
            masks[i, k] = (
                col_fits
                & (key_row >= row_first)
                & (key_row < row_first + NA_ROWS)
                & (doc_row == doc_col)
            )
    for layer, out_ref in enumerate(out_refs):

        def per_head(h, carry, layer=layer, out_ref=out_ref):
            lines = [table_ref[layer, h, r : r + 1, :] for r in range(table_ref.shape[2])]
            tiles = []
            for r in range(len(lines) - 1):
                line = lines[r] + pltpu.roll(lines[r + 1], GRID_W, 1)
                line = jnp.broadcast_to(line, shape)
                tiles.append(
                    pltpu.roll(line, LANES - (NA_COLS - 1), 1, stride=1, stride_axis=0)
                )
            for i in range(rows_dev):
                rows = slice(i * GRID_W, (i + 1) * GRID_W)
                for k in range(3 * tiles_side):
                    tile = tiles[2 * k - i + NA_ROWS - 1 - HALF_ROWS]
                    out_ref[h, rows, k * LANES : (k + 1) * LANES] = jnp.where(
                        masks[i, k], tile, MASKED
                    )
            return carry

        lax.fori_loop(0, out_ref.shape[0], per_head, 0)


def prepare(documents, near, far, offset_bias):
    tokens = documents.shape[0]
    total_rows = tokens // GRID_W * lax.axis_size("sp")
    layers, heads, _, cols = offset_bias.shape
    table = jnp.pad(offset_bias, ((0, 0), (0, 0), (0, 0), (0, LANES - cols)))
    size = heads * tokens * 3 * tokens
    return pl.pallas_call(
        functools.partial(prepare_kernel, total_rows),
        out_shape=[jax.ShapeDtypeStruct((heads, tokens, 3 * tokens), jnp.float32)] * layers,
        in_specs=[VMEM] * 4,
        out_specs=[VMEM] * layers,
        name="prepare",
        compiler_params=pltpu.CompilerParams(vmem_limit_bytes=16 * 2**20),
        cost_estimate=pl.CostEstimate(
            flops=4 * layers * size, bytes_accessed=layers * size * 4, transcendentals=0
        ),
    )(documents.reshape(1, tokens), near.reshape(1, tokens), far.reshape(1, tokens), table)


def scale_kernel(first_layer, tokens, *refs):
    if first_layer:
        x_ref, gain_ref, scaled_ref, inverse_ref = refs
    else:
        x_ref, total_ref, gain_ref, scaled_ref, inverse_ref, own_ref, new = refs
    parts, _, width = x_ref.shape
    if not first_layer:
        squares = jnp.zeros((tokens, 1), jnp.float32)
        for j in range(parts):
            total = total_ref[j].astype(jnp.float32)
            squares += jnp.sum(total * total, axis=1, keepdims=True)
        out_inverse = lax.rsqrt(squares / D + EPS)
    squares = jnp.zeros((tokens, 1), jnp.float32)
    for j in range(parts):
        x = x_ref[j, :tokens, :].astype(jnp.float32)
        if not first_layer:
            post = x_ref[j, tokens : tokens + PAD_ROWS, :].astype(jnp.float32)
            post = post[0:1] + post[1:2] + post[2:3]
            x = x + total_ref[j].astype(jnp.float32) * out_inverse * post
            rounded = x.astype(jnp.bfloat16)
            new[j] = rounded
            x = rounded.astype(jnp.float32)
        squares += jnp.sum(x * x, axis=1, keepdims=True)
        scaled_ref[:, j * width : (j + 1) * width] = (x * gain_ref[j]).astype(jnp.bfloat16)
    inverse_ref[...] = lax.rsqrt(squares / D + EPS)
    if not first_layer:
        own_ref[...] = new[lax.axis_index("tp")]


def scale(x_all, total_all, gain, tokens):
    first_layer = total_all is None
    parts, _, width = x_all.shape
    outs = [
        jax.ShapeDtypeStruct((tokens, parts * width), jnp.bfloat16),
        jax.ShapeDtypeStruct((tokens, 1), jnp.float32),
    ]
    args, scratch = [x_all], []
    if not first_layer:
        outs.append(jax.ShapeDtypeStruct((tokens, width), jnp.bfloat16))
        scratch.append(pltpu.VMEM((parts, tokens, width), jnp.bfloat16))
        args.append(total_all)
    args.append(gain.reshape(parts, 1, width))
    return pl.pallas_call(
        functools.partial(scale_kernel, first_layer, tokens),
        out_shape=outs,
        in_specs=[VMEM] * len(args),
        out_specs=[VMEM] * len(outs),
        scratch_shapes=scratch,
        name="scale",
        compiler_params=pltpu.CompilerParams(vmem_limit_bytes=8 * 2**20),
        cost_estimate=pl.CostEstimate(
            flops=8 * tokens * parts * width,
            bytes_accessed=4 * tokens * parts * width * 2,
            transcendentals=tokens,
        ),
    )(*args)


def project_kernel(places, firsts, factor, scaled_ref, inverse_ref, *refs):
    if len(firsts) > 1:
        w_refs, (out_ref, w_other, w_all) = refs[:-3], refs[-3:]
        place_weights(places, w_refs, w_other, firsts[1])
    else:
        w_refs, (out_ref, w_all) = refs[:-2], refs[-2:]
    place_weights(places, w_refs, w_all, firsts[0])
    product = jnp.dot(scaled_ref[...], w_all[...], preferred_element_type=jnp.float32)
    product = (product * inverse_ref[...]).astype(jnp.bfloat16)
    if factor is not None:
        product = product * jnp.asarray(factor, jnp.bfloat16)
    out_ref[...] = product


def project(scaled, inverse, weights, part, columns, firsts, width, factor=None):
    tokens = scaled.shape[0]
    blocks = [w for _, _, w in weights]
    rows = weight_rows(weights)
    outs = [jax.ShapeDtypeStruct((tokens, width), jnp.bfloat16)]
    outs += [jax.ShapeDtypeStruct((rows, width), jnp.bfloat16)] * (len(firsts) - 1)
    return pl.pallas_call(
        functools.partial(project_kernel, weight_places(weights), firsts, factor),
        grid=(1,),
        out_shape=outs,
        in_specs=[VMEM] * 2
        + [
            pl.BlockSpec((*w.shape[:2], columns), lambda i: (0, 0, part)) for w in blocks
        ],
        out_specs=[VMEM] * len(outs),
        scratch_shapes=[pltpu.VMEM((rows, width), jnp.bfloat16)],
        name="project",
        compiler_params=pltpu.CompilerParams(vmem_limit_bytes=16 * 2**20),
        cost_estimate=pl.CostEstimate(
            flops=2 * tokens * rows * width,
            bytes_accessed=2 * rows * width * 2,
            transcendentals=0,
        ),
    )(scaled, inverse, *blocks)


def attend_kernel(q_ref, own_ref, near_ref, far_ref, bias_ref, w_ref, out_ref):
    tokens, width = q_ref.shape
    odd = lax.rem(lax.axis_index("sp"), 2)
    sides = ((own_ref, 1), (near_ref, 2 - 2 * odd), (far_ref, 2 * odd))
    lane = lax.broadcasted_iota(jnp.int32, (tokens, LANES), 1)
    lower = lane < HEAD_DIM
    attended = []
    for pair in range(width // LANES):
        lanes = slice(pair * LANES, (pair + 1) * LANES)
        value_lanes = slice(width + pair * LANES, width + (pair + 1) * LANES)
        queries = q_ref[:, lanes]
        results = []
        for half in range(2):
            chosen = jnp.where(lower if half == 0 else ~lower, queries, 0)
            head = 2 * pair + half
            scores = []
            for side, block in sides:
                start = pl.multiple_of(block * tokens, LANES)
                scores.append(
                    lax.dot_general(
                        chosen,
                        side[:, lanes],
                        (((1,), (1,)), ((), ())),
                        preferred_element_type=jnp.float32,
                    )
                    + bias_ref[head, :, pl.ds(start, tokens)]
                )
            top = jnp.max(
                jnp.maximum(jnp.maximum(scores[0], scores[1]), scores[2]),
                axis=1,
                keepdims=True,
            )
            exps = [jnp.exp(score - top) for score in scores]
            total = jnp.sum(exps[0] + exps[1] + exps[2], axis=1, keepdims=True)
            mixed = sum(
                jnp.dot(
                    e.astype(jnp.bfloat16),
                    side[:, value_lanes],
                    preferred_element_type=jnp.float32,
                )
                for e, (side, _) in zip(exps, sides)
            )
            results.append(mixed / total)
        attended.append(jnp.where(lower, results[0], results[1]).astype(jnp.bfloat16))
    attended = jnp.concatenate(attended, axis=1)
    for n in range(out_ref.shape[0]):
        out_ref[n] = lax.dot_general(
            attended,
            w_ref[n * width : (n + 1) * width, :],
            (((1,), (1,)), ((), ())),
            preferred_element_type=jnp.float32,
        ).astype(jnp.bfloat16)


def attend(queries, own, near, far, bias, w_out):
    tokens, width = queries.shape
    rows = w_out.shape[0]
    heads = width // HEAD_DIM
    return pl.pallas_call(
        attend_kernel,
        out_shape=jax.ShapeDtypeStruct((rows // width, tokens, width), jnp.bfloat16),
        in_specs=[VMEM] * 6,
        out_specs=VMEM,
        name="attend",
        compiler_params=pltpu.CompilerParams(vmem_limit_bytes=20 * 2**20),
        cost_estimate=pl.CostEstimate(
            flops=4 * heads * tokens * 3 * tokens * LANES + 2 * tokens * rows * width,
            bytes_accessed=heads * tokens * 3 * tokens * 4 + rows * width * 2,
            transcendentals=heads * tokens * 3 * tokens,
        ),
    )(queries, own, near, far, bias, w_out)


def summed_kernel(arrived_ref, out_ref):
    total = jnp.sum(arrived_ref[...].astype(jnp.float32), axis=0).astype(jnp.bfloat16)
    for n in range(out_ref.shape[0]):
        out_ref[n] = total


def summed_copies(arrived):
    parts, tokens, width = arrived.shape
    spec = pl.BlockSpec((parts, GRID_W, width), lambda i: (0, i, 0))
    return pl.pallas_call(
        summed_kernel,
        grid=(tokens // GRID_W,),
        out_shape=jax.ShapeDtypeStruct(arrived.shape, arrived.dtype),
        in_specs=[spec],
        out_specs=spec,
        name="summed",
        compiler_params=pltpu.CompilerParams(vmem_limit_bytes=8 * 2**20),
        cost_estimate=pl.CostEstimate(
            flops=2 * parts * tokens * width,
            bytes_accessed=4 * parts * tokens * width,
            transcendentals=0,
        ),
    )(arrived)


def spread_kernel(x_ref, gain_ref, out_ref):
    tokens = x_ref.shape[0]
    rest = gain_ref[...]
    rows = []
    for _ in range(3):
        part = rest.astype(jnp.bfloat16)
        rows.append(part.astype(jnp.float32))
        rest = rest - rows[-1]
    index = lax.broadcasted_iota(jnp.int32, (PAD_ROWS, x_ref.shape[1]), 0)
    tail = jnp.where(index == 0, rows[0], jnp.where(index == 1, rows[1], rows[2]))
    tail = jnp.where(index < 3, tail, 0.0).astype(jnp.bfloat16)
    for n in range(out_ref.shape[0]):
        out_ref[n, :tokens, :] = x_ref[...]
        out_ref[n, tokens:, :] = tail


def spread(x, gain, copies):
    tokens, width = x.shape
    return pl.pallas_call(
        spread_kernel,
        out_shape=jax.ShapeDtypeStruct((copies, tokens + PAD_ROWS, width), x.dtype),
        in_specs=[VMEM] * 2,
        out_specs=VMEM,
        name="spread",
        compiler_params=pltpu.CompilerParams(vmem_limit_bytes=8 * 2**20),
        cost_estimate=pl.CostEstimate(
            flops=0, bytes_accessed=2 * copies * tokens * width, transcendentals=0
        ),
    )(x, gain.reshape(1, width))


def layers(
    stream, documents, q_weight, k_weight, v_weight, out_weight, pre_gain, post_gain, offset_bias
):
    tokens, width = stream.shape

    def side_by_side(layer):
        mats = (k_weight, v_weight, q_weight, out_weight)
        return jnp.concatenate([m[layer] for m in mats], axis=1)

    doc_near, doc_far = partner(documents), across(documents)
    x_copies = spread(stream, post_gain[0], lax.axis_size("tp"))
    x_all = exchange(x_copies, "tp")
    chunk, doc_near, doc_far = lax.optimization_barrier((side_by_side(0), doc_near, doc_far))
    biases = prepare(documents, doc_near, doc_far, offset_bias)
    slots = ring(chunk)
    weights = with_partner(slots)

    def block(layer, scaled, inverse, weights):
        (kv,) = project(scaled, inverse, weights, 0, 2 * width, (0,), 2 * width)
        near = partner(kv)
        far = across(kv)
        queries, w_out = project(
            scaled, inverse, weights, 1, 2 * width, (0, width), width, HEAD_DIM**-0.5
        )
        return attend(queries, kv, near, far, biases[layer], w_out)

    scaled, inverse = scale(x_all, None, pre_gain[0], tokens)
    partial_sums = block(0, scaled, inverse, weights)
    chunk, partial_sums = lax.optimization_barrier(
        (side_by_side(1), partial_sums)
    )
    slots = ring(chunk)
    arrived = exchange(partial_sums, "tp")
    arrived, slots[-2], slots[2] = lax.optimization_barrier((arrived, slots[-2], slots[2]))
    weights = with_partner(slots)
    total_all = exchange(summed_copies(arrived), "tp")
    scaled, inverse, own = scale(x_all, total_all, pre_gain[1], tokens)
    partial_sums = block(1, scaled, inverse, weights)
    own_total = exchange(partial_sums, "tp").astype(jnp.float32).sum(axis=0)
    squares = jnp.sum(own_total * own_total, axis=-1, keepdims=True)
    squares = exchange(copies_for(squares, "tp"), "tp").sum(axis=0)
    out_inverse = lax.rsqrt(squares / D + EPS)
    return (own.astype(jnp.float32) + own_total * out_inverse * post_gain[1]).astype(
        jnp.bfloat16
    )


def solution(mesh):
    in_specs = (
        P(("grp", "sp"), "tp"),
        P(("grp", "sp")),
        P(None, "sp", "tp"),
        P(None, "sp", "tp"),
        P(None, "sp", "tp"),
        P(None, "sp", "tp"),
        P(),
        P(None, "tp"),
        P(None, "tp", None, None),
    )
    out_specs = P(("grp", "sp"), "tp")
    return jax.shard_map(layers, mesh=mesh, in_specs=in_specs, out_specs=out_specs, check_vma=False)
```

profile of v0, /device:TPU:513, one launch (start us, length us, event | category | flops | bytes accessed | tf_op | source)
XLA Modules:
  0.0 212.1 jit_solution(9227100467636267965)
XLA Ops:
  0.0 20.4 %collective-permute-start = (s32[256]{0:T(256)}, s32[256]{0:T(256)S(1)}, u32[]{:S(2)}, u32[]{:S(2)}) collective-permute-start(s32[256]{0:T(256)} %param.10), channel_id=1, source_target_pairs={{0,8},{8,0},{16,24},{24,16},{32,40},{40,32},{48,56},{56,48},{64,72... | collective-permute-start | bytes 3080 | tf_op jit(solution)/shard_map/ppermute | solution.py:37
  20.4 1.9 collective-permute-start.1
  23.1 0.9 copy-done.7
  24.0 1.1 spread.1
  25.1 3.9 %all-to-all-start = ((bf16[8,264,256]{2,1,0:T(8,128)(2,1)}), bf16[8,264,256]{2,1,0:T(8,128)(2,1)S(1)}, u32[]{:S(2)}, u32[]{:S(2)}) async-start(bf16[8,264,256]{2,1,0:T(8,128)(2,1)} %spread.1), calls=%async_computation | async-start | bytes 2162688 | tf_op jit(solution)/shard_map/all_to_all | solution.py:32
  30.6 1.4 collective-permute-start.2
  32.1 6.3 %collective-permute-done.3.refs_2_ = bf16[128,1024]{1,0:T(8,128)(2,1)S(1)} collective-permute-done((bf16[128,1024]{1,0:T(8,128)(2,1)S(1)}, bf16[128,1024]{1,0:T(8,128)(2,1)S(1)}, u32[]{:S(2)}, u32[]{:S(2)}) %collective-permute-start.3) | collective-permute-done | bytes 262176 | tf_op jit(solution)/shard_map/ppermute | solution.py:57
  39.8 5.4 %collective-permute-done.5.refs_4_ = bf16[128,1024]{1,0:T(8,128)(2,1)S(1)} collective-permute-done((bf16[128,1024]{1,0:T(8,128)(2,1)S(1)}, bf16[128,1024]{1,0:T(8,128)(2,1)S(1)}, u32[]{:S(2)}, u32[]{:S(2)}) %collective-permute-start.5) | collective-permute-done | bytes 262176 | tf_op jit(solution)/shard_map/ppermute | solution.py:57
  45.2 3.4 %collective-permute-done.4.refs_3_ = bf16[128,1024]{1,0:T(8,128)(2,1)S(1)} collective-permute-done((bf16[128,1024]{1,0:T(8,128)(2,1)S(1)}, bf16[128,1024]{1,0:T(8,128)(2,1)S(1)}, u32[]{:S(2)}, u32[]{:S(2)}) %collective-permute-start.4) | collective-permute-done | bytes 262176 | tf_op jit(solution)/shard_map/ppermute | solution.py:54
  48.7 0.9 collective-permute-start.6
  49.6 2.7 %collective-permute-start.8 = (bf16[128,1024]{1,0:T(8,128)(2,1)S(1)}, bf16[128,1024]{1,0:T(8,128)(2,1)S(1)}, u32[]{:S(2)}, u32[]{:S(2)}) collective-permute-start(bf16[128,1024]{1,0:T(8,128)(2,1)S(1)} %collective-permute-done.5.refs_4_), channel_id=1, source_target_pairs={{16,0},{24,8},{32,16},{40,24},{48,32},{56,40},{64,48},{72,56},{80,... | collective-permute-start | bytes 786440 | tf_op jit(solution)/shard_map/ppermute | solution.py:57
  52.3 6.3 %collective-permute-done.7.refs_0_ = bf16[128,1024]{1,0:T(8,128)(2,1)S(1)} collective-permute-done((bf16[128,1024]{1,0:T(8,128)(2,1)S(1)}, bf16[128,1024]{1,0:T(8,128)(2,1)S(1)}, u32[]{:S(2)}, u32[]{:S(2)}) %collective-permute-start.7) | collective-permute-done | bytes 262176 | tf_op jit(solution)/shard_map/ppermute | solution.py:54
  58.6 1.1 collective-permute-start.9
  59.7 7.0 %collective-permute-done.10 = bf16[128,1024]{1,0:T(8,128)(2,1)} collective-permute-done((bf16[128,1024]{1,0:T(8,128)(2,1)S(1)}, bf16[128,1024]{1,0:T(8,128)(2,1)}, u32[]{:S(2)}, u32[]{:S(2)}) %collective-permute-start.10) | collective-permute-done | bytes 262176 | tf_op jit(solution)/shard_map/ppermute | solution.py:54
  66.7 1.9 collective-permute-start.11
  69.0 1.1 collective-permute-done.11.refs_5_
  70.1 2.1 %project.5.own_ref = bf16[256,512]{1,0:T(8,128)(2,1)S(1)} custom-call(bf16[256,2048]{1,0:T(8,128)(2,1)S(1)} %get-tuple-element.24.scaled_ref, f32[256,1]{1,0:T(8,128)S(1)} %get-tuple-element.25.inverse_ref, bf16[5,128,1024]{2,1,0:T(8,128)(2,1)S(1)} %stack.4.refs_0_, bf16[5,128,1024]{2,1,0:T(8,128)(2,1)} %collective-permute-done.6.refs_1_, ...), custom_call_target="tpu_custom_call" | custom-call | flops 536870912 | bytes 4194304 | tf_op jit(solution)/shard_map/project/pallas_call | solution.py:273
  72.2 2.0 collective-permute-start.13
  75.3 2.4 %prepare.1 = (f32[4,256,768]{2,1,0:T(8,128)S(1)}, f32[4,256,768]{2,1,0:T(8,128)S(1)}) custom-call(s32[1,256]{1,0:T(1,128)S(1)} %bitcast.26, s32[1,256]{1,0:T(1,128)S(1)} %bitcast.27, s32[1,256]{1,0:T(1,128)S(1)} %bitcast.28, f32[2,4,15,128]{3,2,1,0:T(8,128)S(1)} %pad.4.table_ref), custom_call_target="tpu_custom_call" | custom-call | flops 6291456 | bytes 6291456 | tf_op jit(solution)/shard_map/prepare/pallas_call | solution.py:182
  77.8 1.6 copy-done
  79.4 1.8 project.4
  81.2 3.1 %attend.2 = bf16[8,256,256]{2,1,0:T(8,128)(2,1)} custom-call(bf16[256,256]{1,0:T(8,128)(2,1)S(1)} %get-tuple-element.27.q_ref, bf16[256,512]{1,0:T(8,128)(2,1)S(1)} %project.5.own_ref, bf16[256,512]{1,0:T(8,128)(2,1)S(1)} %collective-permute-done.12.near_ref, bf16[256,512]{1,0:T(8,128)(2,1)S(1)} %collective-permute-done.13.far_ref, ...), custom_call_target="tpu_custom_call" | custom-call | flops 671088640 | bytes 4194304 | tf_op jit(solution)/shard_map/attend/pallas_call | solution.py:351
  84.3 6.8 %all-to-all-start.1 = ((bf16[8,256,256]{2,1,0:T(8,128)(2,1)}), bf16[8,256,256]{2,1,0:T(8,128)(2,1)S(1)}, u32[]{:S(2)}, u32[]{:S(2)}) async-start(bf16[8,256,256]{2,1,0:T(8,128)(2,1)} %attend.2), calls=%async_computation.1 | async-start | bytes 2097152 | tf_op jit(solution)/shard_map/all_to_all | solution.py:32
  91.3 1.9 collective-permute-start.14
  93.2 5.9 %collective-permute-done.16.refs_2_ = bf16[128,1024]{1,0:T(8,128)(2,1)S(1)} collective-permute-done((bf16[128,1024]{1,0:T(8,128)(2,1)S(1)}, bf16[128,1024]{1,0:T(8,128)(2,1)S(1)}, u32[]{:S(2)}, u32[]{:S(2)}) %collective-permute-start.16) | collective-permute-done | bytes 262176 | tf_op jit(solution)/shard_map/ppermute | solution.py:57
  99.1 0.8 collective-permute-start.17
  100.7 5.2 %collective-permute-done.17.refs_4_ = bf16[128,1024]{1,0:T(8,128)(2,1)S(1)} collective-permute-done((bf16[128,1024]{1,0:T(8,128)(2,1)S(1)}, bf16[128,1024]{1,0:T(8,128)(2,1)S(1)}, u32[]{:S(2)}, u32[]{:S(2)}) %collective-permute-start.17) | collective-permute-done | bytes 262176 | tf_op jit(solution)/shard_map/ppermute | solution.py:57
  105.8 1.5 collective-permute-done.15.refs_3_
  107.4 13.0 %all-to-all-done.1.arrived_ref = bf16[8,256,256]{2,1,0:T(8,128)(2,1)S(1)} async-done(((bf16[8,256,256]{2,1,0:T(8,128)(2,1)}), bf16[8,256,256]{2,1,0:T(8,128)(2,1)S(1)}, u32[]{:S(2)}, u32[]{:S(2)}) %all-to-all-start.1) | async-done | bytes 1048608 | tf_op jit(solution)/shard_map/all_to_all | solution.py:32
  120.4 1.7 summed.1
  122.1 4.4 %all-to-all-start.2 = ((bf16[8,256,256]{2,1,0:T(8,128)(2,1)}), bf16[8,256,256]{2,1,0:T(8,128)(2,1)}, u32[]{:S(2)}, u32[]{:S(2)}) async-start(bf16[8,256,256]{2,1,0:T(8,128)(2,1)} %summed.1), calls=%async_computation.2 | async-start | bytes 2097152 | tf_op jit(solution)/shard_map/all_to_all | solution.py:32
  126.6 0.9 copy-done.4
  128.2 1.8 collective-permute-start.19
  130.1 0.8 collective-permute-start.20
  130.9 6.4 %collective-permute-done.19.refs_0_ = bf16[128,1024]{1,0:T(8,128)(2,1)S(1)} collective-permute-done((bf16[128,1024]{1,0:T(8,128)(2,1)S(1)}, bf16[128,1024]{1,0:T(8,128)(2,1)S(1)}, u32[]{:S(2)}, u32[]{:S(2)}) %collective-permute-start.19) | collective-permute-done | bytes 262176 | tf_op jit(solution)/shard_map/ppermute | solution.py:54
  137.9 1.3 collective-permute-start.21
  139.2 6.3 %collective-permute-done.22 = bf16[128,1024]{1,0:T(8,128)(2,1)} collective-permute-done((bf16[128,1024]{1,0:T(8,128)(2,1)S(1)}, bf16[128,1024]{1,0:T(8,128)(2,1)}, u32[]{:S(2)}, u32[]{:S(2)}) %collective-permute-start.22) | collective-permute-done | bytes 262176 | tf_op jit(solution)/shard_map/ppermute | solution.py:54
  145.5 1.8 collective-permute-start.23
  147.3 8.4 %all-to-all-done.2.refs_1_ = bf16[8,256,256]{2,1,0:T(8,128)(2,1)} async-done(((bf16[8,256,256]{2,1,0:T(8,128)(2,1)}), bf16[8,256,256]{2,1,0:T(8,128)(2,1)}, u32[]{:S(2)}, u32[]{:S(2)}) %all-to-all-start.2) | async-done | bytes 1048608 | tf_op jit(solution)/shard_map/all_to_all | solution.py:32
  155.7 2.5 %scale.3 = (bf16[256,2048]{1,0:T(8,128)(2,1)S(1)}, f32[256,1]{1,0:T(8,128)S(1)}, bf16[256,256]{1,0:T(8,128)(2,1)S(1)}) custom-call(bf16[8,264,256]{2,1,0:T(8,128)(2,1)S(1)} %all-to-all-done.refs_0_, bf16[8,256,256]{2,1,0:T(8,128)(2,1)} %all-to-all-done.2.refs_1_, f32[8,1,256]{2,1,0:T(1,128)S(1)} %bitcast.24), custom_call_target="tpu_custom_call" | custom-call | flops 4194304 | bytes 4194304 | tf_op jit(solution)/shard_map/scale/pallas_call | solution.py:237
  158.9 2.1 project.7.own_ref
  160.9 4.2 %collective-permute-start.25 = (bf16[256,512]{1,0:T(8,128)(2,1)S(1)}, bf16[256,512]{1,0:T(8,128)(2,1)S(1)}, u32[]{:S(2)}, u32[]{:S(2)}) collective-permute-start(bf16[256,512]{1,0:T(8,128)(2,1)S(1)} %project.7.own_ref), channel_id=1, source_target_pairs={{8,16},{24,32},{40,48},{56,64},{72,80},{88,96},{104,112},{16,8},{3... | collective-permute-start | bytes 786440 | tf_op jit(solution)/shard_map/ppermute | solution.py:43
  165.3 1.9 project.6
  167.3 1.9 collective-permute-done.25.far_ref
  169.2 2.1 %attend.3 = bf16[8,256,256]{2,1,0:T(8,128)(2,1)S(1)} custom-call(bf16[256,256]{1,0:T(8,128)(2,1)S(1)} %get-tuple-element.40.q_ref, bf16[256,512]{1,0:T(8,128)(2,1)S(1)} %project.7.own_ref, bf16[256,512]{1,0:T(8,128)(2,1)S(1)} %collective-permute-done.24.near_ref, bf16[256,512]{1,0:T(8,128)(2,1)S(1)} %collective-permute-done.25.far_ref, ...), custom_call_target="tpu_custom_call" | custom-call | flops 671088640 | bytes 4194304 | tf_op jit(solution)/shard_map/attend/pallas_call | solution.py:351
  171.4 30.7 %all_to_all.25 = bf16[8,256,256]{2,1,0:T(8,128)(2,1)S(1)} all-to-all(bf16[8,256,256]{2,1,0:T(8,128)(2,1)S(1)} %attend.3), channel_id=1, replica_groups=mesh['grp'=2,'sp'=16,'tp'=8] {'tp'}, dimensions={0} | all-to-all | bytes 2097152 | tf_op jit(solution)/shard_map/all_to_all | solution.py:32
  202.3 9.0 %all_to_all.26 = f32[8,256,1]{1,2,0:T(1,128)S(1)} all-to-all(f32[8,256,1]{1,2,0:T(1,128)S(1)} %broadcast_in_dim.12), channel_id=1, replica_groups=mesh['grp'=2,'sp'=16,'tp'=8] {'tp'}, dimensions={0} | all-to-all | bytes 16384 | tf_op jit(solution)/shard_map/all_to_all | solution.py:32
  211.4 0.8 add_convert_fusion
  (77 shorter events, 8.7 us)
Async XLA Ops:
  0.0 30.5 %collective-permute-start = (s32[256]{0:T(256)}, s32[256]{0:T(256)S(1)}, u32[]{:S(2)}, u32[]{:S(2)}) collective-permute-start(s32[256]{0:T(256)} %param.10), channel_id=1, source_target_pairs={{0,8},{8,0},{16,24},{24,16},{32,40},{40,32},{48,56},{56,48},{64,72... | collective-permute-start | bytes 3080 | tf_op jit(solution)/shard_map/ppermute | solution.py:37
  20.4 10.1 %collective-permute-start.1 = (s32[256]{0:T(256)}, s32[256]{0:T(256)S(1)}, u32[]{:S(2)}, u32[]{:S(2)}) collective-permute-start(s32[256]{0:T(256)} %param.10), channel_id=1, source_target_pairs={{8,16},{24,32},{40,48},{56,64},{72,80},{88,96},{104,112},{16,8},{3... | collective-permute-start | bytes 3080 | tf_op jit(solution)/shard_map/ppermute | solution.py:43
  23.1 0.9 copy-start.7
  25.1 3.9 %copy-start.12 = (bf16[2,128,256]{2,1,0:T(8,128)(2,1)S(1)}, bf16[2,128,256]{2,1,0:T(8,128)(2,1)}, u32[]{:S(2)}) copy-start(bf16[2,128,256]{2,1,0:T(8,128)(2,1)} %param.14) | copy-start | bytes 393220
  25.1 3.9 %copy-start.13 = (bf16[2,128,256]{2,1,0:T(8,128)(2,1)S(1)}, bf16[2,128,256]{2,1,0:T(8,128)(2,1)}, u32[]{:S(2)}) copy-start(bf16[2,128,256]{2,1,0:T(8,128)(2,1)} %param.11) | copy-start | bytes 393220
  25.1 4.6 %copy-start.14 = (bf16[2,128,256]{2,1,0:T(8,128)(2,1)S(1)}, bf16[2,128,256]{2,1,0:T(8,128)(2,1)}, u32[]{:S(2)}) copy-start(bf16[2,128,256]{2,1,0:T(8,128)(2,1)} %param.13) | copy-start | bytes 393220
  25.1 4.6 %copy-start.15 = (bf16[2,128,256]{2,1,0:T(8,128)(2,1)S(1)}, bf16[2,128,256]{2,1,0:T(8,128)(2,1)}, u32[]{:S(2)}) copy-start(bf16[2,128,256]{2,1,0:T(8,128)(2,1)} %param.12) | copy-start | bytes 393220
  25.1 43.4 %all-to-all-start = ((bf16[8,264,256]{2,1,0:T(8,128)(2,1)}), bf16[8,264,256]{2,1,0:T(8,128)(2,1)S(1)}, u32[]{:S(2)}, u32[]{:S(2)}) async-start(bf16[8,264,256]{2,1,0:T(8,128)(2,1)} %spread.1), calls=%async_computation | async-start | bytes 2162688 | tf_op jit(solution)/shard_map/all_to_all | solution.py:32
  30.4 38.1 %copy-start.17 = (f32[2,2048]{1,0:T(2,128)S(1)}, f32[2,2048]{1,0:T(2,128)}, u32[]{:S(2)}) copy-start(f32[2,2048]{1,0:T(2,128)} %param.15) | copy-start | bytes 49156
  30.5 7.9 %collective-permute-start.3 = (bf16[128,1024]{1,0:T(8,128)(2,1)S(1)}, bf16[128,1024]{1,0:T(8,128)(2,1)S(1)}, u32[]{:S(2)}, u32[]{:S(2)}) collective-permute-start(bf16[128,1024]{1,0:T(8,128)(2,1)S(1)} %pad_maximum_fusion.1.refs_0_), channel_id=1, source_target_pairs={{16,0},{24,8},{32,16},{40,24},{48,32},{56,40},{64,48},{72,56},{80,... | collective-permute-start | bytes 786440 | tf_op jit(solution)/shard_map/ppermute | solution.py:57
  30.6 8.8 %collective-permute-start.2 = (bf16[128,1024]{1,0:T(8,128)(2,1)S(1)}, bf16[128,1024]{1,0:T(8,128)(2,1)S(1)}, u32[]{:S(2)}, u32[]{:S(2)}) collective-permute-start(bf16[128,1024]{1,0:T(8,128)(2,1)S(1)} %pad_maximum_fusion.1.refs_0_), channel_id=1, source_target_pairs={{0,16},{8,24},{16,32},{24,40},{32,48},{40,56},{48,64},{56,72},{64,... | collective-permute-start | bytes 786440 | tf_op jit(solution)/shard_map/ppermute | solution.py:54
  38.3 6.9 %collective-permute-start.5 = (bf16[128,1024]{1,0:T(8,128)(2,1)S(1)}, bf16[128,1024]{1,0:T(8,128)(2,1)S(1)}, u32[]{:S(2)}, u32[]{:S(2)}) collective-permute-start(bf16[128,1024]{1,0:T(8,128)(2,1)S(1)} %collective-permute-done.3.refs_2_), channel_id=1, source_target_pairs={{16,0},{24,8},{32,16},{40,24},{48,32},{56,40},{64,48},{72,56},{80,... | collective-permute-start | bytes 786440 | tf_op jit(solution)/shard_map/ppermute | solution.py:57
  39.4 9.2 %collective-permute-start.4 = (bf16[128,1024]{1,0:T(8,128)(2,1)S(1)}, bf16[128,1024]{1,0:T(8,128)(2,1)S(1)}, u32[]{:S(2)}, u32[]{:S(2)}) collective-permute-start(bf16[128,1024]{1,0:T(8,128)(2,1)S(1)} %collective-permute-done.2.refs_1_), channel_id=1, source_target_pairs={{0,16},{8,24},{16,32},{24,40},{32,48},{40,56},{48,64},{56,72},{64,... | collective-permute-start | bytes 786440 | tf_op jit(solution)/shard_map/ppermute | solution.py:54
  48.7 21.3 %collective-permute-start.6 = (bf16[5,128,1024]{2,1,0:T(8,128)(2,1)S(1)}, bf16[5,128,1024]{2,1,0:T(8,128)(2,1)}, u32[]{:S(2)}, u32[]{:S(2)}) collective-permute-start(bf16[5,128,1024]{2,1,0:T(8,128)(2,1)S(1)} %stack.4.refs_0_), channel_id=1, source_target_pairs={{0,8},{8,0},{16,24},{24,16},{32,40},{40,32},{48,56},{56,48},{64,72... | collective-permute-start | bytes 3932168 | tf_op jit(solution)/shard_map/ppermute | solution.py:37
  49.6 8.9 %collective-permute-start.7 = (bf16[128,1024]{1,0:T(8,128)(2,1)S(1)}, bf16[128,1024]{1,0:T(8,128)(2,1)S(1)}, u32[]{:S(2)}, u32[]{:S(2)}) collective-permute-start(bf16[128,1024]{1,0:T(8,128)(2,1)S(1)} %collective-permute-done.4.refs_3_), channel_id=1, source_target_pairs={{0,16},{8,24},{16,32},{24,40},{32,48},{40,56},{48,64},{56,72},{64,... | collective-permute-start | bytes 786440 | tf_op jit(solution)/shard_map/ppermute | solution.py:54
  49.6 8.9 %collective-permute-start.8 = (bf16[128,1024]{1,0:T(8,128)(2,1)S(1)}, bf16[128,1024]{1,0:T(8,128)(2,1)S(1)}, u32[]{:S(2)}, u32[]{:S(2)}) collective-permute-start(bf16[128,1024]{1,0:T(8,128)(2,1)S(1)} %collective-permute-done.5.refs_4_), channel_id=1, source_target_pairs={{16,0},{24,8},{32,16},{40,24},{48,32},{56,40},{64,48},{72,56},{80,... | collective-permute-start | bytes 786440 | tf_op jit(solution)/shard_map/ppermute | solution.py:57
  58.5 8.2 %collective-permute-start.10 = (bf16[128,1024]{1,0:T(8,128)(2,1)S(1)}, bf16[128,1024]{1,0:T(8,128)(2,1)}, u32[]{:S(2)}, u32[]{:S(2)}) collective-permute-start(bf16[128,1024]{1,0:T(8,128)(2,1)S(1)} %collective-permute-done.7.refs_0_), channel_id=1, source_target_pairs={{0,16},{8,24},{16,32},{24,40},{32,48},{40,56},{48,64},{56,72},{64,... | collective-permute-start | bytes 786440 | tf_op jit(solution)/shard_map/ppermute | solution.py:54
  58.6 10.4 %collective-permute-start.9 = (bf16[2,128,1024]{2,1,0:T(8,128)(2,1)S(1)}, bf16[2,128,1024]{2,1,0:T(8,128)(2,1)S(1)}, u32[]{:S(2)}, u32[]{:S(2)}) collective-permute-start(bf16[2,128,1024]{2,1,0:T(8,128)(2,1)S(1)} %stack.5.refs_2_), channel_id=1, source_target_pairs={{0,8},{8,0},{16,24},{24,16},{32,40},{40,32},{48,56},{56,48},{64,72... | collective-permute-start | bytes 1572872 | tf_op jit(solution)/shard_map/ppermute | solution.py:37
  66.7 3.4 %collective-permute-start.11 = (bf16[1,128,1024]{2,1,0:T(8,128)(2,1)}, bf16[1,128,1024]{2,1,0:T(8,128)(2,1)}, u32[]{:S(2)}, u32[]{:S(2)}) collective-permute-start(bf16[1,128,1024]{2,1,0:T(8,128)(2,1)} %bitcast.9.refs_4_), channel_id=1, source_target_pairs={{0,8},{8,0},{16,24},{24,16},{32,40},{40,32},{48,56},{56,48},{64,72... | collective-permute-start | bytes 786440 | tf_op jit(solution)/shard_map/ppermute | solution.py:37
  70.1 4.5 %copy-start.16 = (f32[2,4,15,31]{3,1,2,0:T(4,128)S(1)}, f32[2,4,15,31]{3,1,2,0:T(4,128)}, u32[]{:S(2)}) copy-start(f32[2,4,15,31]{3,1,2,0:T(4,128)} %param.17) | copy-start | bytes 44644
  70.1 4.5 %copy-start.9 = (bf16[128,256]{1,0:T(8,128)(2,1)S(1)}, bf16[128,256]{1,0:T(8,128)(2,1)}, u32[]{:S(2)}) copy-start(bf16[128,256]{1,0:T(8,128)(2,1)} %get-tuple-element.55) | copy-start | bytes 196612
  70.1 4.5 %copy-start.10 = (bf16[128,256]{1,0:T(8,128)(2,1)S(1)}, bf16[128,256]{1,0:T(8,128)(2,1)}, u32[]{:S(2)}) copy-start(bf16[128,256]{1,0:T(8,128)(2,1)} %get-tuple-element.46) | copy-start | bytes 196612
  70.1 4.5 %copy-start.11 = (bf16[128,256]{1,0:T(8,128)(2,1)S(1)}, bf16[128,256]{1,0:T(8,128)(2,1)}, u32[]{:S(2)}) copy-start(bf16[128,256]{1,0:T(8,128)(2,1)} %get-tuple-element.57) | copy-start | bytes 196612
  70.1 5.3 %copy-start.8 = (s32[256]{0:T(256)S(1)}, s32[256]{0:T(256)}, u32[]{:S(2)}) copy-start(s32[256]{0:T(256)} %param.10) | copy-start | bytes 3076
  72.2 9.0 %collective-permute-start.13 = (bf16[256,512]{1,0:T(8,128)(2,1)S(1)}, bf16[256,512]{1,0:T(8,128)(2,1)S(1)}, u32[]{:S(2)}, u32[]{:S(2)}) collective-permute-start(bf16[256,512]{1,0:T(8,128)(2,1)S(1)} %project.5.own_ref), channel_id=1, source_target_pairs={{8,16},{24,32},{40,48},{56,64},{72,80},{88,96},{104,112},{16,8},{3... | collective-permute-start | bytes 786440 | tf_op jit(solution)/shard_map/ppermute | solution.py:43
  74.2 7.0 %collective-permute-start.12 = (bf16[256,512]{1,0:T(8,128)(2,1)S(1)}, bf16[256,512]{1,0:T(8,128)(2,1)S(1)}, u32[]{:S(2)}, u32[]{:S(2)}) collective-permute-start(bf16[256,512]{1,0:T(8,128)(2,1)S(1)} %project.5.own_ref), channel_id=1, source_target_pairs={{0,8},{8,0},{16,24},{24,16},{32,40},{40,32},{48,56},{56,48},{64,72... | collective-permute-start | bytes 786440 | tf_op jit(solution)/shard_map/ppermute | solution.py:37
  77.7 1.6 copy-start
  84.3 6.8 %copy-start.2 = (bf16[128,1024]{1,0:T(8,128)(2,1)S(1)}, bf16[128,1024]{1,0:T(8,128)(2,1)}, u32[]{:S(2)}) copy-start(bf16[128,1024]{1,0:T(8,128)(2,1)} %pad_maximum_fusion.refs_0_) | copy-start | bytes 786436
  84.3 36.1 %all-to-all-start.1 = ((bf16[8,256,256]{2,1,0:T(8,128)(2,1)}), bf16[8,256,256]{2,1,0:T(8,128)(2,1)S(1)}, u32[]{:S(2)}, u32[]{:S(2)}) async-start(bf16[8,256,256]{2,1,0:T(8,128)(2,1)} %attend.2), calls=%async_computation.1 | async-start | bytes 2097152 | tf_op jit(solution)/shard_map/all_to_all | solution.py:32
  91.2 7.9 %collective-permute-start.16 = (bf16[128,1024]{1,0:T(8,128)(2,1)S(1)}, bf16[128,1024]{1,0:T(8,128)(2,1)S(1)}, u32[]{:S(2)}, u32[]{:S(2)}) collective-permute-start(bf16[128,1024]{1,0:T(8,128)(2,1)S(1)} %copy-done.2), channel_id=1, source_target_pairs={{16,0},{24,8},{32,16},{40,24},{48,32},{56,40},{64,48},{72,56},{80,... | collective-permute-start | bytes 786440 | tf_op jit(solution)/shard_map/ppermute | solution.py:57
  91.3 8.6 %collective-permute-start.14 = (bf16[128,1024]{1,0:T(8,128)(2,1)S(1)}, bf16[128,1024]{1,0:T(8,128)(2,1)S(1)}, u32[]{:S(2)}, u32[]{:S(2)}) collective-permute-start(bf16[128,1024]{1,0:T(8,128)(2,1)S(1)} %copy-done.2), channel_id=1, source_target_pairs={{0,16},{8,24},{16,32},{24,40},{32,48},{40,56},{48,64},{56,72},{64,... | collective-permute-start | bytes 786440 | tf_op jit(solution)/shard_map/ppermute | solution.py:54
  99.1 6.7 %collective-permute-start.17 = (bf16[128,1024]{1,0:T(8,128)(2,1)S(1)}, bf16[128,1024]{1,0:T(8,128)(2,1)S(1)}, u32[]{:S(2)}, u32[]{:S(2)}) collective-permute-start(bf16[128,1024]{1,0:T(8,128)(2,1)S(1)} %collective-permute-done.16.refs_2_), channel_id=1, source_target_pairs={{16,0},{24,8},{32,16},{40,24},{48,32},{56,40},{64,48},{72,56},{80,... | collective-permute-start | bytes 786440 | tf_op jit(solution)/shard_map/ppermute | solution.py:57
  99.9 7.5 %collective-permute-start.15 = (bf16[128,1024]{1,0:T(8,128)(2,1)S(1)}, bf16[128,1024]{1,0:T(8,128)(2,1)S(1)}, u32[]{:S(2)}, u32[]{:S(2)}) collective-permute-start(bf16[128,1024]{1,0:T(8,128)(2,1)S(1)} %collective-permute-done.14.refs_1_), channel_id=1, source_target_pairs={{0,16},{8,24},{16,32},{24,40},{32,48},{40,56},{48,64},{56,72},{64,... | collective-permute-start | bytes 786440 | tf_op jit(solution)/shard_map/ppermute | solution.py:54
  107.4 14.7 %copy-start.3 = (bf16[128,1024]{1,0:T(8,128)(2,1)}, bf16[128,1024]{1,0:T(8,128)(2,1)S(1)}, u32[]{:S(2)}) copy-start(bf16[128,1024]{1,0:T(8,128)(2,1)S(1)} %collective-permute-done.15.refs_3_) | copy-start | bytes 786436
  122.1 33.6 %all-to-all-start.2 = ((bf16[8,256,256]{2,1,0:T(8,128)(2,1)}), bf16[8,256,256]{2,1,0:T(8,128)(2,1)}, u32[]{:S(2)}, u32[]{:S(2)}) async-start(bf16[8,256,256]{2,1,0:T(8,128)(2,1)} %summed.1), calls=%async_computation.2 | async-start | bytes 2097152 | tf_op jit(solution)/shard_map/all_to_all | solution.py:32
  126.6 1.0 copy-start.4
  127.6 31.3 %collective-permute-start.18 = (bf16[5,128,1024]{2,1,0:T(8,128)(2,1)S(1)}, bf16[5,128,1024]{2,1,0:T(8,128)(2,1)}, u32[]{:S(2)}, u32[]{:S(2)}) collective-permute-start(bf16[5,128,1024]{2,1,0:T(8,128)(2,1)S(1)} %stack.6.refs_0_), channel_id=1, source_target_pairs={{0,8},{8,0},{16,24},{24,16},{32,40},{40,32},{48,56},{56,48},{64,72... | collective-permute-start | bytes 3932168 | tf_op jit(solution)/shard_map/ppermute | solution.py:37
  128.2 9.0 %collective-permute-start.19 = (bf16[128,1024]{1,0:T(8,128)(2,1)S(1)}, bf16[128,1024]{1,0:T(8,128)(2,1)S(1)}, u32[]{:S(2)}, u32[]{:S(2)}) collective-permute-start(bf16[128,1024]{1,0:T(8,128)(2,1)S(1)} %copy-done.4), channel_id=1, source_target_pairs={{0,16},{8,24},{16,32},{24,40},{32,48},{40,56},{48,64},{56,72},{64,... | collective-permute-start | bytes 786440 | tf_op jit(solution)/shard_map/ppermute | solution.py:54
  130.1 7.8 %collective-permute-start.20 = (bf16[128,1024]{1,0:T(8,128)(2,1)S(1)}, bf16[128,1024]{1,0:T(8,128)(2,1)S(1)}, u32[]{:S(2)}, u32[]{:S(2)}) collective-permute-start(bf16[128,1024]{1,0:T(8,128)(2,1)S(1)} %collective-permute-done.17.refs_4_), channel_id=1, source_target_pairs={{16,0},{24,8},{32,16},{40,24},{48,32},{56,40},{64,48},{72,56},{80,... | collective-permute-start | bytes 786440 | tf_op jit(solution)/shard_map/ppermute | solution.py:57
  137.3 8.3 %collective-permute-start.22 = (bf16[128,1024]{1,0:T(8,128)(2,1)S(1)}, bf16[128,1024]{1,0:T(8,128)(2,1)}, u32[]{:S(2)}, u32[]{:S(2)}) collective-permute-start(bf16[128,1024]{1,0:T(8,128)(2,1)S(1)} %collective-permute-done.19.refs_0_), channel_id=1, source_target_pairs={{0,16},{8,24},{16,32},{24,40},{32,48},{40,56},{48,64},{56,72},{64,... | collective-permute-start | bytes 786440 | tf_op jit(solution)/shard_map/ppermute | solution.py:54
  137.9 20.9 %collective-permute-start.21 = (bf16[2,128,1024]{2,1,0:T(8,128)(2,1)S(1)}, bf16[2,128,1024]{2,1,0:T(8,128)(2,1)S(1)}, u32[]{:S(2)}, u32[]{:S(2)}) collective-permute-start(bf16[2,128,1024]{2,1,0:T(8,128)(2,1)S(1)} %stack.7.refs_2_), channel_id=1, source_target_pairs={{0,8},{8,0},{16,24},{24,16},{32,40},{40,32},{48,56},{56,48},{64,72... | collective-permute-start | bytes 1572872 | tf_op jit(solution)/shard_map/ppermute | solution.py:37
  145.5 13.3 %collective-permute-start.23 = (bf16[1,128,1024]{2,1,0:T(8,128)(2,1)}, bf16[1,128,1024]{2,1,0:T(8,128)(2,1)}, u32[]{:S(2)}, u32[]{:S(2)}) collective-permute-start(bf16[1,128,1024]{2,1,0:T(8,128)(2,1)} %bitcast.14.refs_4_), channel_id=1, source_target_pairs={{0,8},{8,0},{16,24},{24,16},{32,40},{40,32},{48,56},{56,48},{64,72... | collective-permute-start | bytes 786440 | tf_op jit(solution)/shard_map/ppermute | solution.py:37
  158.2 0.7 copy-start.5
  160.9 8.2 %collective-permute-start.25 = (bf16[256,512]{1,0:T(8,128)(2,1)S(1)}, bf16[256,512]{1,0:T(8,128)(2,1)S(1)}, u32[]{:S(2)}, u32[]{:S(2)}) collective-permute-start(bf16[256,512]{1,0:T(8,128)(2,1)S(1)} %project.7.own_ref), channel_id=1, source_target_pairs={{8,16},{24,32},{40,48},{56,64},{72,80},{88,96},{104,112},{16,8},{3... | collective-permute-start | bytes 786440 | tf_op jit(solution)/shard_map/ppermute | solution.py:43
  165.1 4.0 %collective-permute-start.24 = (bf16[256,512]{1,0:T(8,128)(2,1)S(1)}, bf16[256,512]{1,0:T(8,128)(2,1)S(1)}, u32[]{:S(2)}, u32[]{:S(2)}) collective-permute-start(bf16[256,512]{1,0:T(8,128)(2,1)S(1)} %project.7.own_ref), channel_id=1, source_target_pairs={{0,8},{8,0},{16,24},{24,16},{32,40},{40,32},{48,56},{56,48},{64,72... | collective-permute-start | bytes 786440 | tf_op jit(solution)/shard_map/ppermute | solution.py:37
  165.3 3.9 %copy-start.1 = (f32[4,256,768]{2,1,0:T(8,128)S(1)}, f32[4,256,768]{2,1,0:T(8,128)}, u32[]{:S(2)}) copy-start(f32[4,256,768]{2,1,0:T(8,128)} %copy-done) | copy-start | bytes 9437188
  202.0 9.3 %copy-start.6 = (bf16[256,256]{1,0:T(8,128)(2,1)S(1)}, bf16[256,256]{1,0:T(8,128)(2,1)}, u32[]{:S(2)}) copy-start(bf16[256,256]{1,0:T(8,128)(2,1)} %copy-done.5) | copy-start | bytes 393220
where the time goes:
time: 213 us; the launch traced here: 212 us
  waiting for transfers between devices  78.7 us (37%)
  starting transfers between devices  63.7 us (30%)
  blocking collectives  39.7 us (19%)
  Pallas kernels  21.6 us (10%)
  local copies, waits for them, and re-layouts  6.31 us (3%)
    all_to_all x2, blocking collectives, exchange(): return lax.all_to_all(x, axis, split_axis=0, concat_axis=0, tiled=True)  39.7 us
    ppermute x8, waiting for transfers between devices, ring(): left = lax.ppermute(left, 'sp', up)  31.5 us
    ppermute x9, starting transfers between devices, partner(): return lax.ppermute(x, 'sp', [(i, i ^ 1) for i in range(count)])  28.4 us
    ppermute x6, waiting for transfers between devices, ring(): right = lax.ppermute(right, 'sp', down)  22.8 us
    all_to_all x3, waiting for transfers between devices, exchange(): return lax.all_to_all(x, axis, split_axis=0, concat_axis=0, tiled=True)  21.4 us
    all_to_all x3, starting transfers between devices, exchange(): return lax.all_to_all(x, axis, split_axis=0, concat_axis=0, tiled=True)  15.2 us
    ppermute x3, starting transfers between devices, across(): return lax.ppermute(x, 'sp', moves + [(j, i) for i, j in moves])  8.08 us
    pallas_call x4, Pallas kernels, project(): pl.pallas_call(functools.partial(project_kernel, weight_places(weights),...  7.96 us
  transfers between devices with their start and end apart: 29, of which 15 were waited for; matrix products, arithmetic and copies ran while one was open for 1% of the time, Pallas kernels for 5%

commit v1 on v0

--- a/solution.py
+++ b/solution.py
@@ -43,6 +43,29 @@
     return lax.ppermute(x, "sp", moves + [(j, i) for i, j in moves])
 
 
+def chunk_kernel(*refs):
+    *in_refs, out_ref = refs
+    width = in_refs[0].shape[2]
+    for n, ref in enumerate(in_refs):
+        out_ref[:, n * width : (n + 1) * width] = ref[0]
+
+
+def side_by_side(layer, *mats):
+    _, rows, width = mats[0].shape
+    return pl.pallas_call(
+        chunk_kernel,
+        grid=(1,),
+        out_shape=jax.ShapeDtypeStruct((rows, len(mats) * width), mats[0].dtype),
+        in_specs=[pl.BlockSpec((1, rows, width), lambda i: (layer, 0, 0))] * len(mats),
+        out_specs=pl.BlockSpec((rows, len(mats) * width), lambda i: (0, 0)),
+        name="chunk",
+        compiler_params=pltpu.CompilerParams(vmem_limit_bytes=8 * 2**20),
+        cost_estimate=pl.CostEstimate(
+            flops=0, bytes_accessed=4 * len(mats) * rows * width, transcendentals=0
+        ),
+    )(*mats)
+
+
 def ring(chunk):
     count = lax.axis_size("sp")
     half = count // 2
@@ -50,12 +73,14 @@
     down = [(j, i) for i, j in up]
     slots = {0: chunk}
     left = right = chunk
-    for k in range(1, half // 2 + 1):
+    last = half // 2
+    middle = chunk.shape[0] // 2
+    for k in range(1, last + 1):
+        if k == last:
+            left, right = left[:middle], right[middle:]
         left = lax.ppermute(left, "sp", up)
-        slots[-k] = left
-        if k < half - half // 2:
-            right = lax.ppermute(right, "sp", down)
-            slots[k] = right
+        right = lax.ppermute(right, "sp", down)
+        slots[-k], slots[k] = left, right
     return slots
 
 
@@ -86,8 +111,7 @@
     weights = []
     for low, high in ((0, 2), (3, 3), (4, 4)):
         keys = tuple(k for k in sorted(slots, key=abs) if low <= abs(k) <= high)
-        own = [slots[k] for k in keys]
-        own = stacked(own) if len(own) > 1 else own[0][None]
+        own = stacked([slots[k] for k in keys])
         weights += [(keys, 0, own), (keys, 1, partner(own))]
     return weights
 
@@ -105,12 +129,14 @@
     pairs = lax.axis_size("sp") // 2
     place, parity = me // 2, lax.rem(me, 2)
     width = w_all.shape[1]
+    block_rows = w_all.shape[0] // (2 * pairs)
     for (keys, other), ref in zip(places, refs):
         rows = ref.shape[1]
         for n, k in enumerate(keys):
             block = lax.rem(place + k + pairs, pairs) * 2
             block += 1 - parity if other else parity
-            start = pl.multiple_of(block * rows, rows)
+            offset = block_rows - rows if k > 0 else 0
+            start = pl.multiple_of(block * block_rows + offset, rows)
             w_all[pl.ds(start, rows), :] = ref[n, :, first : first + width]
 
 
@@ -192,12 +218,12 @@
     )(documents.reshape(1, tokens), near.reshape(1, tokens), far.reshape(1, tokens), table)
 
 
-def scale_kernel(first_layer, tokens, *refs):
+def scale_kernel(first_layer, *refs):
     if first_layer:
         x_ref, gain_ref, scaled_ref, inverse_ref = refs
     else:
-        x_ref, total_ref, gain_ref, scaled_ref, inverse_ref, own_ref, new = refs
-    parts, _, width = x_ref.shape
+        x_ref, post_ref, total_ref, gain_ref, scaled_ref, inverse_ref, own_ref, new = refs
+    parts, tokens, width = x_ref.shape
     if not first_layer:
         squares = jnp.zeros((tokens, 1), jnp.float32)
         for j in range(parts):
@@ -206,9 +232,9 @@
         out_inverse = lax.rsqrt(squares / D + EPS)
     squares = jnp.zeros((tokens, 1), jnp.float32)
     for j in range(parts):
-        x = x_ref[j, :tokens, :].astype(jnp.float32)
+        x = x_ref[j].astype(jnp.float32)
         if not first_layer:
-            post = x_ref[j, tokens : tokens + PAD_ROWS, :].astype(jnp.float32)
+            post = post_ref[j].astype(jnp.float32)
             post = post[0:1] + post[1:2] + post[2:3]
             x = x + total_ref[j].astype(jnp.float32) * out_inverse * post
             rounded = x.astype(jnp.bfloat16)
@@ -224,21 +250,33 @@
 def scale(x_all, total_all, gain, tokens):
     first_layer = total_all is None
     parts, _, width = x_all.shape
+    step = GRID_W
     outs = [
         jax.ShapeDtypeStruct((tokens, parts * width), jnp.bfloat16),
         jax.ShapeDtypeStruct((tokens, 1), jnp.float32),
     ]
+    out_specs = [
+        pl.BlockSpec((step, parts * width), lambda i: (i, 0)),
+        pl.BlockSpec((step, 1), lambda i: (i, 0)),
+    ]
     args, scratch = [x_all], []
+    block = pl.BlockSpec((parts, step, width), lambda i: (0, i, 0))
+    in_specs = [block]
     if not first_layer:
         outs.append(jax.ShapeDtypeStruct((tokens, width), jnp.bfloat16))
-        scratch.append(pltpu.VMEM((parts, tokens, width), jnp.bfloat16))
-        args.append(total_all)
+        out_specs.append(pl.BlockSpec((step, width), lambda i: (i, 0)))
+        scratch.append(pltpu.VMEM((parts, step, width), jnp.bfloat16))
+        args += [x_all, total_all]
+        rows = pl.BlockSpec((parts, PAD_ROWS, width), lambda i: (0, tokens // PAD_ROWS, 0))
+        in_specs += [rows, block]
     args.append(gain.reshape(parts, 1, width))
-    return pl.pallas_call(
-        functools.partial(scale_kernel, first_layer, tokens),
+    in_specs.append(pl.BlockSpec((parts, 1, width), lambda i: (0, 0, 0)))
+    return pl.pallas_call(
+        functools.partial(scale_kernel, first_layer),
+        grid=(tokens // step,),
         out_shape=outs,
-        in_specs=[VMEM] * len(args),
-        out_specs=[VMEM] * len(outs),
+        in_specs=in_specs,
+        out_specs=out_specs,
         scratch_shapes=scratch,
         name="scale",
         compiler_params=pltpu.CompilerParams(vmem_limit_bytes=8 * 2**20),
@@ -424,14 +462,11 @@
 ):
     tokens, width = stream.shape
 
-    def side_by_side(layer):
-        mats = (k_weight, v_weight, q_weight, out_weight)
-        return jnp.concatenate([m[layer] for m in mats], axis=1)
-
+    mats = (k_weight, v_weight, q_weight, out_weight)
     doc_near, doc_far = partner(documents), across(documents)
     x_copies = spread(stream, post_gain[0], lax.axis_size("tp"))
     x_all = exchange(x_copies, "tp")
-    chunk, doc_near, doc_far = lax.optimization_barrier((side_by_side(0), doc_near, doc_far))
+    chunk, doc_near, doc_far = lax.optimization_barrier((side_by_side(0, *mats), doc_near, doc_far))
     biases = prepare(documents, doc_near, doc_far, offset_bias)
     slots = ring(chunk)
     weights = with_partner(slots)
@@ -448,7 +483,7 @@
     scaled, inverse = scale(x_all, None, pre_gain[0], tokens)
     partial_sums = block(0, scaled, inverse, weights)
     chunk, partial_sums = lax.optimization_barrier(
-        (side_by_side(1), partial_sums)
+        (side_by_side(1, *mats), partial_sums)
     )
     slots = ring(chunk)
     arrived = exchange(partial_sums, "tp")

time: 213 us -> 210 us (0.986)
  waiting for transfers between devices: 78.7 us -> 73.3 us
  starting transfers between devices: 63.7 us -> 66 us
    ppermute x8, waiting for transfers between devices: 31.5 us -> 8.83 us  [ring(): left = lax.ppermute(left, 'sp', up)]
    ppermute x6 -> x8, waiting for transfers between devices: 22.8 us -> 39.1 us  [ring(): right = lax.ppermute(right, 'sp', down)]
    ppermute x9, starting transfers between devices: 28.4 us -> 24.9 us  [partner(): return lax.ppermute(x, 'sp', [(i, i ^ 1) for i in range(count)])]
    all_to_all x3, starting transfers between devices: 15.2 us -> 18.4 us  [exchange(): return lax.all_to_all(x, axis, split_axis=0, concat_axis=0, tiled=True)]
    ppermute x3, waiting for transfers between devices: 1.93 us -> 4.83 us  [across(): return lax.ppermute(x, 'sp', moves + [(j, i) for i, j in moves])]
    ppermute x8, starting transfers between devices: 6.93 us -> 9.68 us  [ring(): left = lax.ppermute(left, 'sp', up)]
    unnamed x37 -> x41, local copies, waits for them, and re-layouts: 4.18 us -> 5.14 us
    ppermute x6 -> x8, starting transfers between devices: 5.12 us -> 4.84 us  [ring(): right = lax.ppermute(right, 'sp', down)]
  transfers between devices with their start and end apart: 29 -> 31, of which waited for: 15 -> 18; matrix products, arithmetic and copies ran while one was open for 1% -> 0% of each run, Pallas kernels for 5% -> 5%
where the time goes in v1:
time: 210 us; the launch traced here: 209 us
  waiting for transfers between devices  73.3 us (35%)
  starting transfers between devices  66 us (31%)
  blocking collectives  39.7 us (19%)
  Pallas kernels  22.9 us (11%)
  local copies, waits for them, and re-layouts  5.96 us (3%)
    all_to_all x2, blocking collectives, exchange(): return lax.all_to_all(x, axis, split_axis=0, concat_axis=0, tiled=True)  39.7 us
    ppermute x8, waiting for transfers between devices, ring(): right = lax.ppermute(right, 'sp', down)  39.1 us
    ppermute x9, starting transfers between devices, partner(): return lax.ppermute(x, 'sp', [(i, i ^ 1) for i in range(count)])  24.9 us
    all_to_all x3, waiting for transfers between devices, exchange(): return lax.all_to_all(x, axis, split_axis=0, concat_axis=0, tiled=True)  20.2 us
    all_to_all x3, starting transfers between devices, exchange(): return lax.all_to_all(x, axis, split_axis=0, concat_axis=0, tiled=True)  18.4 us
    ppermute x8, starting transfers between devices, ring(): left = lax.ppermute(left, 'sp', up)  9.68 us
    ppermute x8, waiting for transfers between devices, ring(): left = lax.ppermute(left, 'sp', up)  8.83 us
    ppermute x3, starting transfers between devices, across(): return lax.ppermute(x, 'sp', moves + [(j, i) for i, j in moves])  8.07 us
  transfers between devices with their start and end apart: 31, of which 18 were waited for; matrix products, arithmetic and copies ran while one was open for 0% of the time, Pallas kernels for 5%

profile of v1, /device:TPU:513, one launch (start us, length us, event | category | flops | bytes accessed | tf_op | source)
XLA Modules:
  0.0 209.3 jit_solution(2502361955356790665)
XLA Ops:
  1.7 1.1 spread.1
  2.8 8.0 %all-to-all-start = ((bf16[8,264,256]{2,1,0:T(8,128)(2,1)}), bf16[8,264,256]{2,1,0:T(8,128)(2,1)S(1)}, u32[]{:S(2)}, u32[]{:S(2)}) async-start(bf16[8,264,256]{2,1,0:T(8,128)(2,1)} %spread.1), calls=%async_computation | async-start | bytes 2162688 | tf_op jit(solution)/shard_map/all_to_all | solution.py:32
  10.8 16.5 %collective-permute-start = (s32[256]{0:T(256)S(1)}, s32[256]{0:T(256)S(1)}, u32[]{:S(2)}, u32[]{:S(2)}) collective-permute-start(s32[256]{0:T(256)S(1)} %copy-done.17), channel_id=1, source_target_pairs={{0,8},{8,0},{16,24},{24,16},{32,40},{40,32},{48,56},{56,48},{64,72... | collective-permute-start | bytes 3080 | tf_op jit(solution)/shard_map/ppermute | solution.py:37
  27.2 1.9 collective-permute-start.1
  29.3 2.9 %collective-permute-done.1 = s32[256]{0:T(256)S(1)} collective-permute-done((s32[256]{0:T(256)S(1)}, s32[256]{0:T(256)S(1)}, u32[]{:S(2)}, u32[]{:S(2)}) %collective-permute-start.1) | collective-permute-done | bytes 1056 | tf_op jit(solution)/shard_map/ppermute | solution.py:43
  32.2 1.5 collective-permute-start.2
  33.6 5.7 %collective-permute-done.3.refs_2_ = bf16[128,1024]{1,0:T(8,128)(2,1)S(1)} collective-permute-done((bf16[128,1024]{1,0:T(8,128)(2,1)S(1)}, bf16[128,1024]{1,0:T(8,128)(2,1)S(1)}, u32[]{:S(2)}, u32[]{:S(2)}) %collective-permute-start.3) | collective-permute-done | bytes 262176 | tf_op jit(solution)/shard_map/ppermute | solution.py:82
  39.4 1.7 collective-permute-start.4
  41.1 6.3 %collective-permute-done.5.refs_4_ = bf16[128,1024]{1,0:T(8,128)(2,1)S(1)} collective-permute-done((bf16[128,1024]{1,0:T(8,128)(2,1)S(1)}, bf16[128,1024]{1,0:T(8,128)(2,1)S(1)}, u32[]{:S(2)}, u32[]{:S(2)}) %collective-permute-start.5) | collective-permute-done | bytes 262176 | tf_op jit(solution)/shard_map/ppermute | solution.py:82
  47.4 0.9 collective-permute-done.4.refs_3_
  49.0 1.5 collective-permute-start.7
  50.4 6.3 %collective-permute-done.8.refs_1_ = bf16[128,1024]{1,0:T(8,128)(2,1)S(1)} collective-permute-done((bf16[128,1024]{1,0:T(8,128)(2,1)S(1)}, bf16[128,1024]{1,0:T(8,128)(2,1)S(1)}, u32[]{:S(2)}, u32[]{:S(2)}) %collective-permute-start.8) | collective-permute-done | bytes 262176 | tf_op jit(solution)/shard_map/ppermute | solution.py:82
  56.7 1.4 collective-permute-start.11
  58.5 1.7 collective-permute-start.9
  60.6 2.6 %collective-permute-done.10.refs_0_ = bf16[64,1024]{1,0:T(8,128)(2,1)S(1)} collective-permute-done((bf16[64,1024]{1,0:T(8,128)(2,1)S(1)}, bf16[64,1024]{1,0:T(8,128)(2,1)S(1)}, u32[]{:S(2)}, u32[]{:S(2)}) %collective-permute-start.10) | collective-permute-done | bytes 131104 | tf_op jit(solution)/shard_map/ppermute | solution.py:81
  63.3 2.5 %collective-permute-start.12 = (bf16[2,64,1024]{2,1,0:T(8,128)(2,1)S(1)}, bf16[2,64,1024]{2,1,0:T(8,128)(2,1)S(1)}, u32[]{:S(2)}, u32[]{:S(2)}) collective-permute-start(bf16[2,64,1024]{2,1,0:T(8,128)(2,1)S(1)} %stack.8.refs_4_), channel_id=1, source_target_pairs={{0,8},{8,0},{16,24},{24,16},{32,40},{40,32},{48,56},{56,48},{64,72... | collective-permute-start | bytes 786440 | tf_op jit(solution)/shard_map/ppermute | solution.py:37
  67.0 2.3 %project.5.own_ref = bf16[256,512]{1,0:T(8,128)(2,1)S(1)} custom-call(bf16[256,2048]{1,0:T(8,128)(2,1)S(1)} %get-tuple-element.24.scaled_ref, f32[256,1]{1,0:T(8,128)S(1)} %get-tuple-element.25.inverse_ref, bf16[5,128,1024]{2,1,0:T(8,128)(2,1)S(1)} %stack.6.refs_0_, bf16[5,128,1024]{2,1,0:T(8,128)(2,1)} %collective-permute-done.6.refs_1_, ...), custom_call_target="tpu_custom_call" | custom-call | flops 536870912 | bytes 4194304 | tf_op jit(solution)/shard_map/project/pallas_call | solution.py:311
  69.3 2.0 collective-permute-start.14
  71.7 2.4 %prepare.1 = (f32[4,256,768]{2,1,0:T(8,128)S(1)}, f32[4,256,768]{2,1,0:T(8,128)S(1)}) custom-call(s32[1,256]{1,0:T(1,128)S(1)} %bitcast.8, s32[1,256]{1,0:T(1,128)S(1)} %bitcast.9, s32[1,256]{1,0:T(1,128)S(1)} %bitcast.10, f32[2,4,15,128]{3,2,1,0:T(8,128)S(1)} %pad.4.table_ref), custom_call_target="tpu_custom_call" | custom-call | flops 6291456 | bytes 6291456 | tf_op jit(solution)/shard_map/prepare/pallas_call | solution.py:208
  74.1 1.6 copy-done
  75.7 0.9 copy-done.3
  76.7 1.8 project.4
  78.5 3.1 %attend.2 = bf16[8,256,256]{2,1,0:T(8,128)(2,1)} custom-call(bf16[256,256]{1,0:T(8,128)(2,1)S(1)} %get-tuple-element.27.q_ref, bf16[256,512]{1,0:T(8,128)(2,1)S(1)} %project.5.own_ref, bf16[256,512]{1,0:T(8,128)(2,1)S(1)} %collective-permute-done.13.near_ref, bf16[256,512]{1,0:T(8,128)(2,1)S(1)} %collective-permute-done.14.far_ref, ...), custom_call_target="tpu_custom_call" | custom-call | flops 671088640 | bytes 4194304 | tf_op jit(solution)/shard_map/attend/pallas_call | solution.py:389
  81.6 6.0 %all-to-all-start.1 = ((bf16[8,256,256]{2,1,0:T(8,128)(2,1)}), bf16[8,256,256]{2,1,0:T(8,128)(2,1)S(1)}, u32[]{:S(2)}, u32[]{:S(2)}) async-start(bf16[8,256,256]{2,1,0:T(8,128)(2,1)} %attend.2), calls=%async_computation.1 | async-start | bytes 2097152 | tf_op jit(solution)/shard_map/all_to_all | solution.py:32
  87.7 1.9 collective-permute-start.15
  89.6 5.9 %collective-permute-done.17.refs_2_ = bf16[128,1024]{1,0:T(8,128)(2,1)S(1)} collective-permute-done((bf16[128,1024]{1,0:T(8,128)(2,1)S(1)}, bf16[128,1024]{1,0:T(8,128)(2,1)S(1)}, u32[]{:S(2)}, u32[]{:S(2)}) %collective-permute-start.17) | collective-permute-done | bytes 262176 | tf_op jit(solution)/shard_map/ppermute | solution.py:82
  97.1 5.1 %collective-permute-done.18.refs_4_ = bf16[128,1024]{1,0:T(8,128)(2,1)S(1)} collective-permute-done((bf16[128,1024]{1,0:T(8,128)(2,1)S(1)}, bf16[128,1024]{1,0:T(8,128)(2,1)S(1)}, u32[]{:S(2)}, u32[]{:S(2)}) %collective-permute-start.18) | collective-permute-done | bytes 262176 | tf_op jit(solution)/shard_map/ppermute | solution.py:82
  102.1 1.6 collective-permute-done.16.refs_3_
  103.8 13.1 %all-to-all-done.1.arrived_ref = bf16[8,256,256]{2,1,0:T(8,128)(2,1)S(1)} async-done(((bf16[8,256,256]{2,1,0:T(8,128)(2,1)}), bf16[8,256,256]{2,1,0:T(8,128)(2,1)S(1)}, u32[]{:S(2)}, u32[]{:S(2)}) %all-to-all-start.1) | async-done | bytes 1048608 | tf_op jit(solution)/shard_map/all_to_all | solution.py:32
  116.9 1.7 summed.1
  118.6 4.4 %all-to-all-start.2 = ((bf16[8,256,256]{2,1,0:T(8,128)(2,1)}), bf16[8,256,256]{2,1,0:T(8,128)(2,1)}, u32[]{:S(2)}, u32[]{:S(2)}) async-start(bf16[8,256,256]{2,1,0:T(8,128)(2,1)} %summed.1), calls=%async_computation.2 | async-start | bytes 2097152 | tf_op jit(solution)/shard_map/all_to_all | solution.py:32
  123.0 0.9 copy-done.13
  124.7 1.8 collective-permute-start.20
  126.5 6.6 %collective-permute-done.21.refs_1_ = bf16[128,1024]{1,0:T(8,128)(2,1)S(1)} collective-permute-done((bf16[128,1024]{1,0:T(8,128)(2,1)S(1)}, bf16[128,1024]{1,0:T(8,128)(2,1)S(1)}, u32[]{:S(2)}, u32[]{:S(2)}) %collective-permute-start.21) | collective-permute-done | bytes 262176 | tf_op jit(solution)/shard_map/ppermute | solution.py:82
  133.5 1.3 collective-permute-start.22
  134.8 2.6 %collective-permute-start.24 = (bf16[64,1024]{1,0:T(8,128)(2,1)S(1)}, bf16[64,1024]{1,0:T(8,128)(2,1)S(1)}, u32[]{:S(2)}, u32[]{:S(2)}) collective-permute-start(bf16[64,1024]{1,0:T(8,128)(2,1)S(1)} %slice.35), channel_id=1, source_target_pairs={{16,0},{24,8},{32,16},{40,24},{48,32},{56,40},{64,48},{72,56},{80,... | collective-permute-start | bytes 393224 | tf_op jit(solution)/shard_map/ppermute | solution.py:82
  137.6 2.7 %collective-permute-done.24.refs_1_ = bf16[64,1024]{1,0:T(8,128)(2,1)S(1)} collective-permute-done((bf16[64,1024]{1,0:T(8,128)(2,1)S(1)}, bf16[64,1024]{1,0:T(8,128)(2,1)S(1)}, u32[]{:S(2)}, u32[]{:S(2)}) %collective-permute-start.24) | collective-permute-done | bytes 131104 | tf_op jit(solution)/shard_map/ppermute | solution.py:82
  140.2 3.4 %collective-permute-done.23.refs_0_ = bf16[64,1024]{1,0:T(8,128)(2,1)S(1)} collective-permute-done((bf16[64,1024]{1,0:T(8,128)(2,1)S(1)}, bf16[64,1024]{1,0:T(8,128)(2,1)S(1)}, u32[]{:S(2)}, u32[]{:S(2)}) %collective-permute-start.23) | collective-permute-done | bytes 131104 | tf_op jit(solution)/shard_map/ppermute | solution.py:81
  143.6 1.4 collective-permute-start.25
  145.0 7.1 %all-to-all-done.2.refs_2_ = bf16[8,256,256]{2,1,0:T(8,128)(2,1)} async-done(((bf16[8,256,256]{2,1,0:T(8,128)(2,1)}), bf16[8,256,256]{2,1,0:T(8,128)(2,1)}, u32[]{:S(2)}, u32[]{:S(2)}) %all-to-all-start.2) | async-done | bytes 1048608 | tf_op jit(solution)/shard_map/all_to_all | solution.py:32
  152.1 3.3 %scale.3 = (bf16[256,2048]{1,0:T(8,128)(2,1)S(1)}, f32[256,1]{1,0:T(8,128)S(1)}, bf16[256,256]{1,0:T(8,128)(2,1)S(1)}) custom-call(bf16[8,264,256]{2,1,0:T(8,128)(2,1)S(1)} %all-to-all-done.refs_0_.refs_1_, bf16[8,264,256]{2,1,0:T(8,128)(2,1)S(1)} %all-to-all-done.refs_0_.refs_1_, bf16[8,256,256]{2,1,0:T(8,128)(2,1)} %all-to-all-done.2.refs_2_, ...), custom_call_target="tpu_custom_call" | custom-call | flops 4194304 | bytes 4194304 | tf_op jit(solution)/shard_map/scale/pallas_call | solution.py:274
  156.1 2.0 project.7.own_ref
  158.1 4.2 %collective-permute-start.27 = (bf16[256,512]{1,0:T(8,128)(2,1)S(1)}, bf16[256,512]{1,0:T(8,128)(2,1)S(1)}, u32[]{:S(2)}, u32[]{:S(2)}) collective-permute-start(bf16[256,512]{1,0:T(8,128)(2,1)S(1)} %project.7.own_ref), channel_id=1, source_target_pairs={{8,16},{24,32},{40,48},{56,64},{72,80},{88,96},{104,112},{16,8},{3... | collective-permute-start | bytes 786440 | tf_op jit(solution)/shard_map/ppermute | solution.py:43
  162.5 1.9 project.6
  164.4 1.9 collective-permute-done.27.far_ref
  166.4 2.2 %attend.3 = bf16[8,256,256]{2,1,0:T(8,128)(2,1)S(1)} custom-call(bf16[256,256]{1,0:T(8,128)(2,1)S(1)} %get-tuple-element.40.q_ref, bf16[256,512]{1,0:T(8,128)(2,1)S(1)} %project.7.own_ref, bf16[256,512]{1,0:T(8,128)(2,1)S(1)} %collective-permute-done.26.near_ref, bf16[256,512]{1,0:T(8,128)(2,1)S(1)} %collective-permute-done.27.far_ref, ...), custom_call_target="tpu_custom_call" | custom-call | flops 671088640 | bytes 4194304 | tf_op jit(solution)/shard_map/attend/pallas_call | solution.py:389
  168.5 30.6 %all_to_all.25 = bf16[8,256,256]{2,1,0:T(8,128)(2,1)S(1)} all-to-all(bf16[8,256,256]{2,1,0:T(8,128)(2,1)S(1)} %attend.3), channel_id=1, replica_groups=mesh['grp'=2,'sp'=16,'tp'=8] {'tp'}, dimensions={0} | all-to-all | bytes 2097152 | tf_op jit(solution)/shard_map/all_to_all | solution.py:32
  199.5 9.0 %all_to_all.26 = f32[8,256,1]{1,2,0:T(1,128)S(1)} all-to-all(f32[8,256,1]{1,2,0:T(1,128)S(1)} %broadcast_in_dim.4), channel_id=1, replica_groups=mesh['grp'=2,'sp'=16,'tp'=8] {'tp'}, dimensions={0} | all-to-all | bytes 16384 | tf_op jit(solution)/shard_map/all_to_all | solution.py:32
  (89 shorter events, 9.5 us)
Async XLA Ops:
  2.8 8.0 %copy-start.17 = (s32[256]{0:T(256)S(1)}, s32[256]{0:T(256)}, u32[]{:S(2)}) copy-start(s32[256]{0:T(256)} %param.10) | copy-start | bytes 3076
  2.8 26.4 %copy-start.4 = (bf16[2,128,256]{2,1,0:T(8,128)(2,1)S(1)}, bf16[2,128,256]{2,1,0:T(8,128)(2,1)}, u32[]{:S(2)}) copy-start(bf16[2,128,256]{2,1,0:T(8,128)(2,1)} %refs_0_.3) | copy-start | bytes 393220
  2.8 26.4 %copy-start.6 = (bf16[2,128,256]{2,1,0:T(8,128)(2,1)S(1)}, bf16[2,128,256]{2,1,0:T(8,128)(2,1)}, u32[]{:S(2)}) copy-start(bf16[2,128,256]{2,1,0:T(8,128)(2,1)} %refs_1_.3) | copy-start | bytes 393220
  2.8 26.4 %copy-start.8 = (bf16[2,128,256]{2,1,0:T(8,128)(2,1)S(1)}, bf16[2,128,256]{2,1,0:T(8,128)(2,1)}, u32[]{:S(2)}) copy-start(bf16[2,128,256]{2,1,0:T(8,128)(2,1)} %refs_2_.3) | copy-start | bytes 393220
  2.8 26.5 %copy-start.10 = (bf16[2,128,256]{2,1,0:T(8,128)(2,1)S(1)}, bf16[2,128,256]{2,1,0:T(8,128)(2,1)}, u32[]{:S(2)}) copy-start(bf16[2,128,256]{2,1,0:T(8,128)(2,1)} %refs_3_.3) | copy-start | bytes 393220
  2.8 63.0 %all-to-all-start = ((bf16[8,264,256]{2,1,0:T(8,128)(2,1)}), bf16[8,264,256]{2,1,0:T(8,128)(2,1)S(1)}, u32[]{:S(2)}, u32[]{:S(2)}) async-start(bf16[8,264,256]{2,1,0:T(8,128)(2,1)} %spread.1), calls=%async_computation | async-start | bytes 2162688 | tf_op jit(solution)/shard_map/all_to_all | solution.py:32
  10.8 18.5 %collective-permute-start = (s32[256]{0:T(256)S(1)}, s32[256]{0:T(256)S(1)}, u32[]{:S(2)}, u32[]{:S(2)}) collective-permute-start(s32[256]{0:T(256)S(1)} %copy-done.17), channel_id=1, source_target_pairs={{0,8},{8,0},{16,24},{24,16},{32,40},{40,32},{48,56},{56,48},{64,72... | collective-permute-start | bytes 3080 | tf_op jit(solution)/shard_map/ppermute | solution.py:37
  27.2 4.9 %collective-permute-start.1 = (s32[256]{0:T(256)S(1)}, s32[256]{0:T(256)S(1)}, u32[]{:S(2)}, u32[]{:S(2)}) collective-permute-start(s32[256]{0:T(256)S(1)} %copy-done.17), channel_id=1, source_target_pairs={{8,16},{24,32},{40,48},{56,64},{72,80},{88,96},{104,112},{16,8},{3... | collective-permute-start | bytes 3080 | tf_op jit(solution)/shard_map/ppermute | solution.py:43
  32.2 7.2 %collective-permute-start.3 = (bf16[128,1024]{1,0:T(8,128)(2,1)S(1)}, bf16[128,1024]{1,0:T(8,128)(2,1)S(1)}, u32[]{:S(2)}, u32[]{:S(2)}) collective-permute-start(bf16[128,1024]{1,0:T(8,128)(2,1)S(1)} %chunk.3.refs_0_), channel_id=1, source_target_pairs={{16,0},{24,8},{32,16},{40,24},{48,32},{56,40},{64,48},{72,56},{80,... | collective-permute-start | bytes 786440 | tf_op jit(solution)/shard_map/ppermute | solution.py:82
  32.2 7.2 %collective-permute-start.2 = (bf16[128,1024]{1,0:T(8,128)(2,1)S(1)}, bf16[128,1024]{1,0:T(8,128)(2,1)S(1)}, u32[]{:S(2)}, u32[]{:S(2)}) collective-permute-start(bf16[128,1024]{1,0:T(8,128)(2,1)S(1)} %chunk.3.refs_0_), channel_id=1, source_target_pairs={{0,16},{8,24},{16,32},{24,40},{32,48},{40,56},{48,64},{56,72},{64,... | collective-permute-start | bytes 786440 | tf_op jit(solution)/shard_map/ppermute | solution.py:81
  39.4 8.1 %collective-permute-start.5 = (bf16[128,1024]{1,0:T(8,128)(2,1)S(1)}, bf16[128,1024]{1,0:T(8,128)(2,1)S(1)}, u32[]{:S(2)}, u32[]{:S(2)}) collective-permute-start(bf16[128,1024]{1,0:T(8,128)(2,1)S(1)} %collective-permute-done.3.refs_2_), channel_id=1, source_target_pairs={{16,0},{24,8},{32,16},{40,24},{48,32},{56,40},{64,48},{72,56},{80,... | collective-permute-start | bytes 786440 | tf_op jit(solution)/shard_map/ppermute | solution.py:82
  39.4 9.0 %collective-permute-start.4 = (bf16[128,1024]{1,0:T(8,128)(2,1)S(1)}, bf16[128,1024]{1,0:T(8,128)(2,1)S(1)}, u32[]{:S(2)}, u32[]{:S(2)}) collective-permute-start(bf16[128,1024]{1,0:T(8,128)(2,1)S(1)} %collective-permute-done.2.refs_1_), channel_id=1, source_target_pairs={{0,16},{8,24},{16,32},{24,40},{32,48},{40,56},{48,64},{56,72},{64,... | collective-permute-start | bytes 786440 | tf_op jit(solution)/shard_map/ppermute | solution.py:81
  48.4 17.3 %copy-start.19 = (f32[2,2048]{1,0:T(2,128)S(1)}, f32[2,2048]{1,0:T(2,128)}, u32[]{:S(2)}) copy-start(f32[2,2048]{1,0:T(2,128)} %param.15) | copy-start | bytes 49156
  48.5 18.5 %collective-permute-start.6 = (bf16[5,128,1024]{2,1,0:T(8,128)(2,1)S(1)}, bf16[5,128,1024]{2,1,0:T(8,128)(2,1)}, u32[]{:S(2)}, u32[]{:S(2)}) collective-permute-start(bf16[5,128,1024]{2,1,0:T(8,128)(2,1)S(1)} %stack.6.refs_0_), channel_id=1, source_target_pairs={{0,8},{8,0},{16,24},{24,16},{32,40},{40,32},{48,56},{56,48},{64,72... | collective-permute-start | bytes 3932168 | tf_op jit(solution)/shard_map/ppermute | solution.py:37
  49.0 7.7 %collective-permute-start.8 = (bf16[128,1024]{1,0:T(8,128)(2,1)S(1)}, bf16[128,1024]{1,0:T(8,128)(2,1)S(1)}, u32[]{:S(2)}, u32[]{:S(2)}) collective-permute-start(bf16[128,1024]{1,0:T(8,128)(2,1)S(1)} %collective-permute-done.5.refs_4_), channel_id=1, source_target_pairs={{16,0},{24,8},{32,16},{40,24},{48,32},{56,40},{64,48},{72,56},{80,... | collective-permute-start | bytes 786440 | tf_op jit(solution)/shard_map/ppermute | solution.py:82
  49.0 9.1 %collective-permute-start.7 = (bf16[128,1024]{1,0:T(8,128)(2,1)S(1)}, bf16[128,1024]{1,0:T(8,128)(2,1)S(1)}, u32[]{:S(2)}, u32[]{:S(2)}) collective-permute-start(bf16[128,1024]{1,0:T(8,128)(2,1)S(1)} %collective-permute-done.4.refs_3_), channel_id=1, source_target_pairs={{0,16},{8,24},{16,32},{24,40},{32,48},{40,56},{48,64},{56,72},{64,... | collective-permute-start | bytes 786440 | tf_op jit(solution)/shard_map/ppermute | solution.py:81
  56.7 3.9 %collective-permute-start.11 = (bf16[64,1024]{1,0:T(8,128)(2,1)S(1)}, bf16[64,1024]{1,0:T(8,128)(2,1)S(1)}, u32[]{:S(2)}, u32[]{:S(2)}) collective-permute-start(bf16[64,1024]{1,0:T(8,128)(2,1)S(1)} %slice.33), channel_id=1, source_target_pairs={{16,0},{24,8},{32,16},{40,24},{48,32},{56,40},{64,48},{72,56},{80,... | collective-permute-start | bytes 393224 | tf_op jit(solution)/shard_map/ppermute | solution.py:82
  58.1 5.1 %collective-permute-start.10 = (bf16[64,1024]{1,0:T(8,128)(2,1)S(1)}, bf16[64,1024]{1,0:T(8,128)(2,1)S(1)}, u32[]{:S(2)}, u32[]{:S(2)}) collective-permute-start(bf16[64,1024]{1,0:T(8,128)(2,1)S(1)} %slice.32), channel_id=1, source_target_pairs={{0,16},{8,24},{16,32},{24,40},{32,48},{40,56},{48,64},{56,72},{64,... | collective-permute-start | bytes 393224 | tf_op jit(solution)/shard_map/ppermute | solution.py:81
  58.5 8.5 %collective-permute-start.9 = (bf16[2,128,1024]{2,1,0:T(8,128)(2,1)S(1)}, bf16[2,128,1024]{2,1,0:T(8,128)(2,1)}, u32[]{:S(2)}, u32[]{:S(2)}) collective-permute-start(bf16[2,128,1024]{2,1,0:T(8,128)(2,1)S(1)} %stack.7.refs_2_), channel_id=1, source_target_pairs={{0,8},{8,0},{16,24},{24,16},{32,40},{40,32},{48,56},{56,48},{64,72... | collective-permute-start | bytes 1572872 | tf_op jit(solution)/shard_map/ppermute | solution.py:37
  63.3 3.7 %collective-permute-start.12 = (bf16[2,64,1024]{2,1,0:T(8,128)(2,1)S(1)}, bf16[2,64,1024]{2,1,0:T(8,128)(2,1)S(1)}, u32[]{:S(2)}, u32[]{:S(2)}) collective-permute-start(bf16[2,64,1024]{2,1,0:T(8,128)(2,1)S(1)} %stack.8.refs_4_), channel_id=1, source_target_pairs={{0,8},{8,0},{16,24},{24,16},{32,40},{40,32},{48,56},{56,48},{64,72... | collective-permute-start | bytes 786440 | tf_op jit(solution)/shard_map/ppermute | solution.py:37
  66.9 2.4 %copy-start.2 = (bf16[2,64,1024]{2,1,0:T(8,128)(2,1)}, bf16[2,64,1024]{2,1,0:T(8,128)(2,1)S(1)}, u32[]{:S(2)}) copy-start(bf16[2,64,1024]{2,1,0:T(8,128)(2,1)S(1)} %collective-permute-done.12.refs_5_) | copy-start | bytes 786436
  66.9 4.6 %copy-start.5 = (bf16[2,128,256]{2,1,0:T(8,128)(2,1)S(1)}, bf16[2,128,256]{2,1,0:T(8,128)(2,1)}, u32[]{:S(2)}) copy-start(bf16[2,128,256]{2,1,0:T(8,128)(2,1)} %refs_0_.3) | copy-start | bytes 393220
  67.0 4.6 %copy-start.7 = (bf16[2,128,256]{2,1,0:T(8,128)(2,1)S(1)}, bf16[2,128,256]{2,1,0:T(8,128)(2,1)}, u32[]{:S(2)}) copy-start(bf16[2,128,256]{2,1,0:T(8,128)(2,1)} %refs_1_.3) | copy-start | bytes 393220
  67.0 4.6 %copy-start.9 = (bf16[2,128,256]{2,1,0:T(8,128)(2,1)S(1)}, bf16[2,128,256]{2,1,0:T(8,128)(2,1)}, u32[]{:S(2)}) copy-start(bf16[2,128,256]{2,1,0:T(8,128)(2,1)} %refs_2_.3) | copy-start | bytes 393220
  67.0 4.6 %copy-start.11 = (bf16[2,128,256]{2,1,0:T(8,128)(2,1)S(1)}, bf16[2,128,256]{2,1,0:T(8,128)(2,1)}, u32[]{:S(2)}) copy-start(bf16[2,128,256]{2,1,0:T(8,128)(2,1)} %refs_3_.3) | copy-start | bytes 393220
  67.0 4.7 %copy-start.18 = (f32[2,4,15,31]{3,1,2,0:T(4,128)S(1)}, f32[2,4,15,31]{3,1,2,0:T(4,128)}, u32[]{:S(2)}) copy-start(f32[2,4,15,31]{3,1,2,0:T(4,128)} %param.17) | copy-start | bytes 44644
  69.3 9.2 %collective-permute-start.14 = (bf16[256,512]{1,0:T(8,128)(2,1)S(1)}, bf16[256,512]{1,0:T(8,128)(2,1)S(1)}, u32[]{:S(2)}, u32[]{:S(2)}) collective-permute-start(bf16[256,512]{1,0:T(8,128)(2,1)S(1)} %project.5.own_ref), channel_id=1, source_target_pairs={{8,16},{24,32},{40,48},{56,64},{72,80},{88,96},{104,112},{16,8},{3... | collective-permute-start | bytes 786440 | tf_op jit(solution)/shard_map/ppermute | solution.py:43
  71.3 7.2 %collective-permute-start.13 = (bf16[256,512]{1,0:T(8,128)(2,1)S(1)}, bf16[256,512]{1,0:T(8,128)(2,1)S(1)}, u32[]{:S(2)}, u32[]{:S(2)}) collective-permute-start(bf16[256,512]{1,0:T(8,128)(2,1)S(1)} %project.5.own_ref), channel_id=1, source_target_pairs={{0,8},{8,0},{16,24},{24,16},{32,40},{40,32},{48,56},{56,48},{64,72... | collective-permute-start | bytes 786440 | tf_op jit(solution)/shard_map/ppermute | solution.py:37
  74.1 1.6 copy-start
  81.6 35.3 %all-to-all-start.1 = ((bf16[8,256,256]{2,1,0:T(8,128)(2,1)}), bf16[8,256,256]{2,1,0:T(8,128)(2,1)S(1)}, u32[]{:S(2)}, u32[]{:S(2)}) async-start(bf16[8,256,256]{2,1,0:T(8,128)(2,1)} %attend.2), calls=%async_computation.1 | async-start | bytes 2097152 | tf_op jit(solution)/shard_map/all_to_all | solution.py:32
  87.6 7.8 %collective-permute-start.17 = (bf16[128,1024]{1,0:T(8,128)(2,1)S(1)}, bf16[128,1024]{1,0:T(8,128)(2,1)S(1)}, u32[]{:S(2)}, u32[]{:S(2)}) collective-permute-start(bf16[128,1024]{1,0:T(8,128)(2,1)S(1)} %chunk.2.refs_0_), channel_id=1, source_target_pairs={{16,0},{24,8},{32,16},{40,24},{48,32},{56,40},{64,48},{72,56},{80,... | collective-permute-start | bytes 786440 | tf_op jit(solution)/shard_map/ppermute | solution.py:82
  87.7 8.6 %collective-permute-start.15 = (bf16[128,1024]{1,0:T(8,128)(2,1)S(1)}, bf16[128,1024]{1,0:T(8,128)(2,1)S(1)}, u32[]{:S(2)}, u32[]{:S(2)}) collective-permute-start(bf16[128,1024]{1,0:T(8,128)(2,1)S(1)} %chunk.2.refs_0_), channel_id=1, source_target_pairs={{0,16},{8,24},{16,32},{24,40},{32,48},{40,56},{48,64},{56,72},{64,... | collective-permute-start | bytes 786440 | tf_op jit(solution)/shard_map/ppermute | solution.py:81
  95.4 6.7 %collective-permute-start.18 = (bf16[128,1024]{1,0:T(8,128)(2,1)S(1)}, bf16[128,1024]{1,0:T(8,128)(2,1)S(1)}, u32[]{:S(2)}, u32[]{:S(2)}) collective-permute-start(bf16[128,1024]{1,0:T(8,128)(2,1)S(1)} %collective-permute-done.17.refs_2_), channel_id=1, source_target_pairs={{16,0},{24,8},{32,16},{40,24},{48,32},{56,40},{64,48},{72,56},{80,... | collective-permute-start | bytes 786440 | tf_op jit(solution)/shard_map/ppermute | solution.py:82
  96.3 22.3 %copy-start.12 = (bf16[128,1024]{1,0:T(8,128)(2,1)}, bf16[128,1024]{1,0:T(8,128)(2,1)S(1)}, u32[]{:S(2)}) copy-start(bf16[128,1024]{1,0:T(8,128)(2,1)S(1)} %collective-permute-done.15.refs_1_) | copy-start | bytes 786436
  96.3 7.5 %collective-permute-start.16 = (bf16[128,1024]{1,0:T(8,128)(2,1)S(1)}, bf16[128,1024]{1,0:T(8,128)(2,1)S(1)}, u32[]{:S(2)}, u32[]{:S(2)}) collective-permute-start(bf16[128,1024]{1,0:T(8,128)(2,1)S(1)} %collective-permute-done.15.refs_1_), channel_id=1, source_target_pairs={{0,16},{8,24},{16,32},{24,40},{32,48},{40,56},{48,64},{56,72},{64,... | collective-permute-start | bytes 786440 | tf_op jit(solution)/shard_map/ppermute | solution.py:81
  118.6 33.5 %all-to-all-start.2 = ((bf16[8,256,256]{2,1,0:T(8,128)(2,1)}), bf16[8,256,256]{2,1,0:T(8,128)(2,1)}, u32[]{:S(2)}, u32[]{:S(2)}) async-start(bf16[8,256,256]{2,1,0:T(8,128)(2,1)} %summed.1), calls=%async_computation.2 | async-start | bytes 2097152 | tf_op jit(solution)/shard_map/all_to_all | solution.py:32
  123.0 1.0 copy-start.13
  124.0 32.0 %collective-permute-start.19 = (bf16[5,128,1024]{2,1,0:T(8,128)(2,1)S(1)}, bf16[5,128,1024]{2,1,0:T(8,128)(2,1)}, u32[]{:S(2)}, u32[]{:S(2)}) collective-permute-start(bf16[5,128,1024]{2,1,0:T(8,128)(2,1)S(1)} %stack.9.refs_0_), channel_id=1, source_target_pairs={{0,8},{8,0},{16,24},{24,16},{32,40},{40,32},{48,56},{56,48},{64,72... | collective-permute-start | bytes 3932168 | tf_op jit(solution)/shard_map/ppermute | solution.py:37
  124.7 8.5 %collective-permute-start.21 = (bf16[128,1024]{1,0:T(8,128)(2,1)S(1)}, bf16[128,1024]{1,0:T(8,128)(2,1)S(1)}, u32[]{:S(2)}, u32[]{:S(2)}) collective-permute-start(bf16[128,1024]{1,0:T(8,128)(2,1)S(1)} %collective-permute-done.18.refs_4_), channel_id=1, source_target_pairs={{16,0},{24,8},{32,16},{40,24},{48,32},{56,40},{64,48},{72,56},{80,... | collective-permute-start | bytes 786440 | tf_op jit(solution)/shard_map/ppermute | solution.py:82
  124.7 8.8 %collective-permute-start.20 = (bf16[128,1024]{1,0:T(8,128)(2,1)S(1)}, bf16[128,1024]{1,0:T(8,128)(2,1)S(1)}, u32[]{:S(2)}, u32[]{:S(2)}) collective-permute-start(bf16[128,1024]{1,0:T(8,128)(2,1)S(1)} %collective-permute-done.16.refs_3_), channel_id=1, source_target_pairs={{0,16},{8,24},{16,32},{24,40},{32,48},{40,56},{48,64},{56,72},{64,... | collective-permute-start | bytes 786440 | tf_op jit(solution)/shard_map/ppermute | solution.py:81
  133.5 22.6 %collective-permute-start.22 = (bf16[2,128,1024]{2,1,0:T(8,128)(2,1)S(1)}, bf16[2,128,1024]{2,1,0:T(8,128)(2,1)}, u32[]{:S(2)}, u32[]{:S(2)}) collective-permute-start(bf16[2,128,1024]{2,1,0:T(8,128)(2,1)S(1)} %stack.10.refs_2_), channel_id=1, source_target_pairs={{0,8},{8,0},{16,24},{24,16},{32,40},{40,32},{48,56},{56,48},{64,72... | collective-permute-start | bytes 1572872 | tf_op jit(solution)/shard_map/ppermute | solution.py:37
  134.8 5.5 %collective-permute-start.24 = (bf16[64,1024]{1,0:T(8,128)(2,1)S(1)}, bf16[64,1024]{1,0:T(8,128)(2,1)S(1)}, u32[]{:S(2)}, u32[]{:S(2)}) collective-permute-start(bf16[64,1024]{1,0:T(8,128)(2,1)S(1)} %slice.35), channel_id=1, source_target_pairs={{16,0},{24,8},{32,16},{40,24},{48,32},{56,40},{64,48},{72,56},{80,... | collective-permute-start | bytes 393224 | tf_op jit(solution)/shard_map/ppermute | solution.py:82
  137.4 6.2 %collective-permute-start.23 = (bf16[64,1024]{1,0:T(8,128)(2,1)S(1)}, bf16[64,1024]{1,0:T(8,128)(2,1)S(1)}, u32[]{:S(2)}, u32[]{:S(2)}) collective-permute-start(bf16[64,1024]{1,0:T(8,128)(2,1)S(1)} %slice.34), channel_id=1, source_target_pairs={{0,16},{8,24},{16,32},{24,40},{32,48},{40,56},{48,64},{56,72},{64,... | collective-permute-start | bytes 393224 | tf_op jit(solution)/shard_map/ppermute | solution.py:81
  143.6 12.5 %collective-permute-start.25 = (bf16[2,64,1024]{2,1,0:T(8,128)(2,1)S(1)}, bf16[2,64,1024]{2,1,0:T(8,128)(2,1)S(1)}, u32[]{:S(2)}, u32[]{:S(2)}) collective-permute-start(bf16[2,64,1024]{2,1,0:T(8,128)(2,1)S(1)} %stack.11.refs_4_), channel_id=1, source_target_pairs={{0,8},{8,0},{16,24},{24,16},{32,40},{40,32},{48,56},{56,48},{64,72... | collective-permute-start | bytes 786440 | tf_op jit(solution)/shard_map/ppermute | solution.py:37
  158.1 8.2 %collective-permute-start.27 = (bf16[256,512]{1,0:T(8,128)(2,1)S(1)}, bf16[256,512]{1,0:T(8,128)(2,1)S(1)}, u32[]{:S(2)}, u32[]{:S(2)}) collective-permute-start(bf16[256,512]{1,0:T(8,128)(2,1)S(1)} %project.7.own_ref), channel_id=1, source_target_pairs={{8,16},{24,32},{40,48},{56,64},{72,80},{88,96},{104,112},{16,8},{3... | collective-permute-start | bytes 786440 | tf_op jit(solution)/shard_map/ppermute | solution.py:43
  162.3 4.0 %collective-permute-start.26 = (bf16[256,512]{1,0:T(8,128)(2,1)S(1)}, bf16[256,512]{1,0:T(8,128)(2,1)S(1)}, u32[]{:S(2)}, u32[]{:S(2)}) collective-permute-start(bf16[256,512]{1,0:T(8,128)(2,1)S(1)} %project.7.own_ref), channel_id=1, source_target_pairs={{0,8},{8,0},{16,24},{24,16},{32,40},{40,32},{48,56},{56,48},{64,72... | collective-permute-start | bytes 786440 | tf_op jit(solution)/shard_map/ppermute | solution.py:37
  162.5 3.9 %copy-start.1 = (f32[4,256,768]{2,1,0:T(8,128)S(1)}, f32[4,256,768]{2,1,0:T(8,128)}, u32[]{:S(2)}) copy-start(f32[4,256,768]{2,1,0:T(8,128)} %copy-done) | copy-start | bytes 9437188
  199.2 9.3 %copy-start.15 = (bf16[256,256]{1,0:T(8,128)(2,1)S(1)}, bf16[256,256]{1,0:T(8,128)(2,1)}, u32[]{:S(2)}) copy-start(bf16[256,256]{1,0:T(8,128)(2,1)} %copy-done.14) | copy-start | bytes 393220
  (3 other events, 2.5 us)

commit v2 on v0

--- a/solution.py
+++ b/solution.py
@@ -50,12 +50,14 @@
     down = [(j, i) for i, j in up]
     slots = {0: chunk}
     left = right = chunk
-    for k in range(1, half // 2 + 1):
+    last = half // 2
+    middle = chunk.shape[0] // 2
+    for k in range(1, last + 1):
+        if k == last:
+            left, right = left[:middle], right[middle:]
         left = lax.ppermute(left, "sp", up)
-        slots[-k] = left
-        if k < half - half // 2:
-            right = lax.ppermute(right, "sp", down)
-            slots[k] = right
+        right = lax.ppermute(right, "sp", down)
+        slots[-k], slots[k] = left, right
     return slots
 
 
@@ -86,8 +88,7 @@
     weights = []
     for low, high in ((0, 2), (3, 3), (4, 4)):
         keys = tuple(k for k in sorted(slots, key=abs) if low <= abs(k) <= high)
-        own = [slots[k] for k in keys]
-        own = stacked(own) if len(own) > 1 else own[0][None]
+        own = stacked([slots[k] for k in keys])
         weights += [(keys, 0, own), (keys, 1, partner(own))]
     return weights
 
@@ -105,12 +106,14 @@
     pairs = lax.axis_size("sp") // 2
     place, parity = me // 2, lax.rem(me, 2)
     width = w_all.shape[1]
+    block_rows = w_all.shape[0] // (2 * pairs)
     for (keys, other), ref in zip(places, refs):
         rows = ref.shape[1]
         for n, k in enumerate(keys):
             block = lax.rem(place + k + pairs, pairs) * 2
             block += 1 - parity if other else parity
-            start = pl.multiple_of(block * rows, rows)
+            offset = block_rows - rows if k > 0 else 0
+            start = pl.multiple_of(block * block_rows + offset, rows)
             w_all[pl.ds(start, rows), :] = ref[n, :, first : first + width]
 
 

time: 213 us -> 210 us (0.986)
  waiting for transfers between devices: 78.7 us -> 74.7 us
    ppermute x8, waiting for transfers between devices: 31.5 us -> 10.3 us  [ring(): left = lax.ppermute(left, 'sp', up)]
    ppermute x6 -> x8, waiting for transfers between devices: 22.8 us -> 39.6 us  [ring(): right = lax.ppermute(right, 'sp', down)]
    ppermute x6 -> x8, starting transfers between devices: 5.12 us -> 3.87 us  [ring(): right = lax.ppermute(right, 'sp', down)]
    unnamed x37 -> x39, local copies, waits for them, and re-layouts: 4.18 us -> 5.13 us
  transfers between devices with their start and end apart: 29 -> 31, of which waited for: 15 -> 18; matrix products, arithmetic and copies ran while one was open for 1% -> 1% of each run, Pallas kernels for 5% -> 5%
where the time goes in v2:
time: 210 us
  waiting for transfers between devices  74.7 us (36%)
  starting transfers between devices  64.9 us (31%)
  blocking collectives  39.7 us (19%)
  Pallas kernels  21.6 us (10%)
  local copies, waits for them, and re-layouts  7.28 us (3%)
    all_to_all x2, blocking collectives, exchange(): return lax.all_to_all(x, axis, split_axis=0, concat_axis=0, tiled=True)  39.7 us
    ppermute x8, waiting for transfers between devices, ring(): right = lax.ppermute(right, 'sp', down)  39.6 us
    ppermute x9, starting transfers between devices, partner(): return lax.ppermute(x, 'sp', [(i, i ^ 1) for i in range(count)])  29 us
    all_to_all x3, waiting for transfers between devices, exchange(): return lax.all_to_all(x, axis, split_axis=0, concat_axis=0, tiled=True)  22.1 us
    all_to_all x3, starting transfers between devices, exchange(): return lax.all_to_all(x, axis, split_axis=0, concat_axis=0, tiled=True)  15 us
    ppermute x8, waiting for transfers between devices, ring(): left = lax.ppermute(left, 'sp', up)  10.3 us
    ppermute x8, starting transfers between devices, ring(): left = lax.ppermute(left, 'sp', up)  8.93 us
    ppermute x3, starting transfers between devices, across(): return lax.ppermute(x, 'sp', moves + [(j, i) for i, j in moves])  8.08 us
  transfers between devices with their start and end apart: 31, of which 18 were waited for; matrix products, arithmetic and copies ran while one was open for 1% of the time, Pallas kernels for 5%

profile of v2, /device:TPU:513, one launch (start us, length us, event | category | flops | bytes accessed | tf_op | source)
XLA Modules:
  0.0 209.7 jit_solution(12357304114333153435)
XLA Ops:
  0.0 20.4 %collective-permute-start = (s32[256]{0:T(256)}, s32[256]{0:T(256)S(1)}, u32[]{:S(2)}, u32[]{:S(2)}) collective-permute-start(s32[256]{0:T(256)} %param.10), channel_id=1, source_target_pairs={{0,8},{8,0},{16,24},{24,16},{32,40},{40,32},{48,56},{56,48},{64,72... | collective-permute-start | bytes 3080 | tf_op jit(solution)/shard_map/ppermute | solution.py:37
  20.4 1.9 collective-permute-start.1
  23.1 0.9 copy-done.8
  24.0 1.1 spread.1
  25.1 3.9 %all-to-all-start = ((bf16[8,264,256]{2,1,0:T(8,128)(2,1)}), bf16[8,264,256]{2,1,0:T(8,128)(2,1)S(1)}, u32[]{:S(2)}, u32[]{:S(2)}) async-start(bf16[8,264,256]{2,1,0:T(8,128)(2,1)} %spread.1), calls=%async_computation | async-start | bytes 2162688 | tf_op jit(solution)/shard_map/all_to_all | solution.py:32
  30.6 1.4 collective-permute-start.2
  32.0 6.3 %collective-permute-done.3.refs_2_ = bf16[128,1024]{1,0:T(8,128)(2,1)S(1)} collective-permute-done((bf16[128,1024]{1,0:T(8,128)(2,1)S(1)}, bf16[128,1024]{1,0:T(8,128)(2,1)S(1)}, u32[]{:S(2)}, u32[]{:S(2)}) %collective-permute-start.3) | collective-permute-done | bytes 262176 | tf_op jit(solution)/shard_map/ppermute | solution.py:59
  39.8 5.4 %collective-permute-done.5.refs_4_ = bf16[128,1024]{1,0:T(8,128)(2,1)S(1)} collective-permute-done((bf16[128,1024]{1,0:T(8,128)(2,1)S(1)}, bf16[128,1024]{1,0:T(8,128)(2,1)S(1)}, u32[]{:S(2)}, u32[]{:S(2)}) %collective-permute-start.5) | collective-permute-done | bytes 262176 | tf_op jit(solution)/shard_map/ppermute | solution.py:59
  45.2 3.4 %collective-permute-done.4.refs_3_ = bf16[128,1024]{1,0:T(8,128)(2,1)S(1)} collective-permute-done((bf16[128,1024]{1,0:T(8,128)(2,1)S(1)}, bf16[128,1024]{1,0:T(8,128)(2,1)S(1)}, u32[]{:S(2)}, u32[]{:S(2)}) %collective-permute-start.4) | collective-permute-done | bytes 262176 | tf_op jit(solution)/shard_map/ppermute | solution.py:58
  49.6 1.5 collective-permute-start.7
  51.0 6.3 %collective-permute-done.8.refs_1_ = bf16[128,1024]{1,0:T(8,128)(2,1)S(1)} collective-permute-done((bf16[128,1024]{1,0:T(8,128)(2,1)S(1)}, bf16[128,1024]{1,0:T(8,128)(2,1)S(1)}, u32[]{:S(2)}, u32[]{:S(2)}) %collective-permute-start.8) | collective-permute-done | bytes 262176 | tf_op jit(solution)/shard_map/ppermute | solution.py:59
  57.3 1.6 collective-permute-start.11
  59.1 1.6 collective-permute-start.9
  61.2 2.8 %collective-permute-done.10.refs_0_ = bf16[64,1024]{1,0:T(8,128)(2,1)S(1)} collective-permute-done((bf16[64,1024]{1,0:T(8,128)(2,1)S(1)}, bf16[64,1024]{1,0:T(8,128)(2,1)S(1)}, u32[]{:S(2)}, u32[]{:S(2)}) %collective-permute-start.10) | collective-permute-done | bytes 131104 | tf_op jit(solution)/shard_map/ppermute | solution.py:58
  64.1 2.3 %collective-permute-start.12 = (bf16[2,64,1024]{2,1,0:T(8,128)(2,1)S(1)}, bf16[2,64,1024]{2,1,0:T(8,128)(2,1)S(1)}, u32[]{:S(2)}, u32[]{:S(2)}) collective-permute-start(bf16[2,64,1024]{2,1,0:T(8,128)(2,1)S(1)} %stack.8.refs_4_), channel_id=1, source_target_pairs={{0,8},{8,0},{16,24},{24,16},{32,40},{40,32},{48,56},{56,48},{64,72... | collective-permute-start | bytes 786440 | tf_op jit(solution)/shard_map/ppermute | solution.py:37
  67.6 2.2 %project.5.own_ref = bf16[256,512]{1,0:T(8,128)(2,1)S(1)} custom-call(bf16[256,2048]{1,0:T(8,128)(2,1)S(1)} %get-tuple-element.24.scaled_ref, f32[256,1]{1,0:T(8,128)S(1)} %get-tuple-element.25.inverse_ref, bf16[5,128,1024]{2,1,0:T(8,128)(2,1)S(1)} %stack.6.refs_0_, bf16[5,128,1024]{2,1,0:T(8,128)(2,1)} %collective-permute-done.6.refs_1_, ...), custom_call_target="tpu_custom_call" | custom-call | flops 536870912 | bytes 4194304 | tf_op jit(solution)/shard_map/project/pallas_call | solution.py:276
  69.8 2.0 collective-permute-start.14
  72.2 2.4 %prepare.1 = (f32[4,256,768]{2,1,0:T(8,128)S(1)}, f32[4,256,768]{2,1,0:T(8,128)S(1)}) custom-call(s32[1,256]{1,0:T(1,128)S(1)} %bitcast.24, s32[1,256]{1,0:T(1,128)S(1)} %bitcast.25, s32[1,256]{1,0:T(1,128)S(1)} %bitcast.26, f32[2,4,15,128]{3,2,1,0:T(8,128)S(1)} %pad.4.table_ref), custom_call_target="tpu_custom_call" | custom-call | flops 6291456 | bytes 6291456 | tf_op jit(solution)/shard_map/prepare/pallas_call | solution.py:185
  74.6 1.6 copy-done
  76.2 0.9 copy-done.3
  77.2 1.8 project.4
  79.0 3.1 %attend.2 = bf16[8,256,256]{2,1,0:T(8,128)(2,1)} custom-call(bf16[256,256]{1,0:T(8,128)(2,1)S(1)} %get-tuple-element.27.q_ref, bf16[256,512]{1,0:T(8,128)(2,1)S(1)} %project.5.own_ref, bf16[256,512]{1,0:T(8,128)(2,1)S(1)} %collective-permute-done.13.near_ref, bf16[256,512]{1,0:T(8,128)(2,1)S(1)} %collective-permute-done.14.far_ref, ...), custom_call_target="tpu_custom_call" | custom-call | flops 671088640 | bytes 4194304 | tf_op jit(solution)/shard_map/attend/pallas_call | solution.py:354
  82.1 6.7 %all-to-all-start.1 = ((bf16[8,256,256]{2,1,0:T(8,128)(2,1)}), bf16[8,256,256]{2,1,0:T(8,128)(2,1)S(1)}, u32[]{:S(2)}, u32[]{:S(2)}) async-start(bf16[8,256,256]{2,1,0:T(8,128)(2,1)} %attend.2), calls=%async_computation.1 | async-start | bytes 2097152 | tf_op jit(solution)/shard_map/all_to_all | solution.py:32
  89.0 1.8 collective-permute-start.15
  90.8 5.9 %collective-permute-done.17.refs_2_ = bf16[128,1024]{1,0:T(8,128)(2,1)S(1)} collective-permute-done((bf16[128,1024]{1,0:T(8,128)(2,1)S(1)}, bf16[128,1024]{1,0:T(8,128)(2,1)S(1)}, u32[]{:S(2)}, u32[]{:S(2)}) %collective-permute-start.17) | collective-permute-done | bytes 262176 | tf_op jit(solution)/shard_map/ppermute | solution.py:59
  96.7 1.0 collective-permute-start.18
  98.3 5.1 %collective-permute-done.18.refs_4_ = bf16[128,1024]{1,0:T(8,128)(2,1)S(1)} collective-permute-done((bf16[128,1024]{1,0:T(8,128)(2,1)S(1)}, bf16[128,1024]{1,0:T(8,128)(2,1)S(1)}, u32[]{:S(2)}, u32[]{:S(2)}) %collective-permute-start.18) | collective-permute-done | bytes 262176 | tf_op jit(solution)/shard_map/ppermute | solution.py:59
  103.4 1.9 collective-permute-done.16.refs_3_
  105.3 12.8 %all-to-all-done.1.arrived_ref = bf16[8,256,256]{2,1,0:T(8,128)(2,1)S(1)} async-done(((bf16[8,256,256]{2,1,0:T(8,128)(2,1)}), bf16[8,256,256]{2,1,0:T(8,128)(2,1)S(1)}, u32[]{:S(2)}, u32[]{:S(2)}) %all-to-all-start.1) | async-done | bytes 1048608 | tf_op jit(solution)/shard_map/all_to_all | solution.py:32
  118.1 1.7 summed.1
  119.7 4.4 %all-to-all-start.2 = ((bf16[8,256,256]{2,1,0:T(8,128)(2,1)}), bf16[8,256,256]{2,1,0:T(8,128)(2,1)}, u32[]{:S(2)}, u32[]{:S(2)}) async-start(bf16[8,256,256]{2,1,0:T(8,128)(2,1)} %summed.1), calls=%async_computation.2 | async-start | bytes 2097152 | tf_op jit(solution)/shard_map/all_to_all | solution.py:32
  124.2 0.9 copy-done.5
  126.0 1.7 collective-permute-start.20
  127.7 6.6 %collective-permute-done.21.refs_1_ = bf16[128,1024]{1,0:T(8,128)(2,1)S(1)} collective-permute-done((bf16[128,1024]{1,0:T(8,128)(2,1)S(1)}, bf16[128,1024]{1,0:T(8,128)(2,1)S(1)}, u32[]{:S(2)}, u32[]{:S(2)}) %collective-permute-start.21) | collective-permute-done | bytes 262176 | tf_op jit(solution)/shard_map/ppermute | solution.py:59
  134.8 1.3 collective-permute-start.22
  136.4 1.5 collective-permute-start.23
  137.8 3.5 %collective-permute-done.24.refs_1_ = bf16[64,1024]{1,0:T(8,128)(2,1)S(1)} collective-permute-done((bf16[64,1024]{1,0:T(8,128)(2,1)S(1)}, bf16[64,1024]{1,0:T(8,128)(2,1)S(1)}, u32[]{:S(2)}, u32[]{:S(2)}) %collective-permute-start.24) | collective-permute-done | bytes 131104 | tf_op jit(solution)/shard_map/ppermute | solution.py:59
  141.3 1.2 collective-permute-done.23.refs_0_
  142.6 1.4 collective-permute-start.25
  144.0 9.3 %all-to-all-done.2.refs_1_ = bf16[8,256,256]{2,1,0:T(8,128)(2,1)} async-done(((bf16[8,256,256]{2,1,0:T(8,128)(2,1)}), bf16[8,256,256]{2,1,0:T(8,128)(2,1)}, u32[]{:S(2)}, u32[]{:S(2)}) %all-to-all-start.2) | async-done | bytes 1048608 | tf_op jit(solution)/shard_map/all_to_all | solution.py:32
  153.3 2.5 %scale.3 = (bf16[256,2048]{1,0:T(8,128)(2,1)S(1)}, f32[256,1]{1,0:T(8,128)S(1)}, bf16[256,256]{1,0:T(8,128)(2,1)S(1)}) custom-call(bf16[8,264,256]{2,1,0:T(8,128)(2,1)S(1)} %all-to-all-done.refs_0_, bf16[8,256,256]{2,1,0:T(8,128)(2,1)} %all-to-all-done.2.refs_1_, f32[8,1,256]{2,1,0:T(1,128)S(1)} %bitcast.22), custom_call_target="tpu_custom_call" | custom-call | flops 4194304 | bytes 4194304 | tf_op jit(solution)/shard_map/scale/pallas_call | solution.py:240
  156.5 2.0 project.7.own_ref
  158.5 4.2 %collective-permute-start.27 = (bf16[256,512]{1,0:T(8,128)(2,1)S(1)}, bf16[256,512]{1,0:T(8,128)(2,1)S(1)}, u32[]{:S(2)}, u32[]{:S(2)}) collective-permute-start(bf16[256,512]{1,0:T(8,128)(2,1)S(1)} %project.7.own_ref), channel_id=1, source_target_pairs={{8,16},{24,32},{40,48},{56,64},{72,80},{88,96},{104,112},{16,8},{3... | collective-permute-start | bytes 786440 | tf_op jit(solution)/shard_map/ppermute | solution.py:43
  162.9 1.9 project.6
  164.8 1.9 collective-permute-done.27.far_ref
  166.8 2.2 %attend.3 = bf16[8,256,256]{2,1,0:T(8,128)(2,1)S(1)} custom-call(bf16[256,256]{1,0:T(8,128)(2,1)S(1)} %get-tuple-element.40.q_ref, bf16[256,512]{1,0:T(8,128)(2,1)S(1)} %project.7.own_ref, bf16[256,512]{1,0:T(8,128)(2,1)S(1)} %collective-permute-done.26.near_ref, bf16[256,512]{1,0:T(8,128)(2,1)S(1)} %collective-permute-done.27.far_ref, ...), custom_call_target="tpu_custom_call" | custom-call | flops 671088640 | bytes 4194304 | tf_op jit(solution)/shard_map/attend/pallas_call | solution.py:354
  168.9 30.7 %all_to_all.25 = bf16[8,256,256]{2,1,0:T(8,128)(2,1)S(1)} all-to-all(bf16[8,256,256]{2,1,0:T(8,128)(2,1)S(1)} %attend.3), channel_id=1, replica_groups=mesh['grp'=2,'sp'=16,'tp'=8] {'tp'}, dimensions={0} | all-to-all | bytes 2097152 | tf_op jit(solution)/shard_map/all_to_all | solution.py:32
  199.9 9.0 %all_to_all.26 = f32[8,256,1]{1,2,0:T(1,128)S(1)} all-to-all(f32[8,256,1]{1,2,0:T(1,128)S(1)} %broadcast_in_dim.4), channel_id=1, replica_groups=mesh['grp'=2,'sp'=16,'tp'=8] {'tp'}, dimensions={0} | all-to-all | bytes 16384 | tf_op jit(solution)/shard_map/all_to_all | solution.py:32
  (89 shorter events, 11.2 us)
Async XLA Ops:
  0.0 30.4 %collective-permute-start = (s32[256]{0:T(256)}, s32[256]{0:T(256)S(1)}, u32[]{:S(2)}, u32[]{:S(2)}) collective-permute-start(s32[256]{0:T(256)} %param.10), channel_id=1, source_target_pairs={{0,8},{8,0},{16,24},{24,16},{32,40},{40,32},{48,56},{56,48},{64,72... | collective-permute-start | bytes 3080 | tf_op jit(solution)/shard_map/ppermute | solution.py:37
  20.4 10.0 %collective-permute-start.1 = (s32[256]{0:T(256)}, s32[256]{0:T(256)S(1)}, u32[]{:S(2)}, u32[]{:S(2)}) collective-permute-start(s32[256]{0:T(256)} %param.10), channel_id=1, source_target_pairs={{8,16},{24,32},{40,48},{56,64},{72,80},{88,96},{104,112},{16,8},{3... | collective-permute-start | bytes 3080 | tf_op jit(solution)/shard_map/ppermute | solution.py:43
  25.1 3.9 %copy-start.13 = (bf16[2,128,256]{2,1,0:T(8,128)(2,1)S(1)}, bf16[2,128,256]{2,1,0:T(8,128)(2,1)}, u32[]{:S(2)}) copy-start(bf16[2,128,256]{2,1,0:T(8,128)(2,1)} %param.14) | copy-start | bytes 393220
  25.1 3.9 %copy-start.14 = (bf16[2,128,256]{2,1,0:T(8,128)(2,1)S(1)}, bf16[2,128,256]{2,1,0:T(8,128)(2,1)}, u32[]{:S(2)}) copy-start(bf16[2,128,256]{2,1,0:T(8,128)(2,1)} %param.11) | copy-start | bytes 393220
  25.1 4.6 %copy-start.15 = (bf16[2,128,256]{2,1,0:T(8,128)(2,1)S(1)}, bf16[2,128,256]{2,1,0:T(8,128)(2,1)}, u32[]{:S(2)}) copy-start(bf16[2,128,256]{2,1,0:T(8,128)(2,1)} %param.13) | copy-start | bytes 393220
  25.1 4.6 %copy-start.16 = (bf16[2,128,256]{2,1,0:T(8,128)(2,1)S(1)}, bf16[2,128,256]{2,1,0:T(8,128)(2,1)}, u32[]{:S(2)}) copy-start(bf16[2,128,256]{2,1,0:T(8,128)(2,1)} %param.12) | copy-start | bytes 393220
  25.1 41.2 %all-to-all-start = ((bf16[8,264,256]{2,1,0:T(8,128)(2,1)}), bf16[8,264,256]{2,1,0:T(8,128)(2,1)S(1)}, u32[]{:S(2)}, u32[]{:S(2)}) async-start(bf16[8,264,256]{2,1,0:T(8,128)(2,1)} %spread.1), calls=%async_computation | async-start | bytes 2162688 | tf_op jit(solution)/shard_map/all_to_all | solution.py:32
  30.5 7.9 %collective-permute-start.3 = (bf16[128,1024]{1,0:T(8,128)(2,1)S(1)}, bf16[128,1024]{1,0:T(8,128)(2,1)S(1)}, u32[]{:S(2)}, u32[]{:S(2)}) collective-permute-start(bf16[128,1024]{1,0:T(8,128)(2,1)S(1)} %pad_maximum_fusion.1.refs_0_), channel_id=1, source_target_pairs={{16,0},{24,8},{32,16},{40,24},{48,32},{56,40},{64,48},{72,56},{80,... | collective-permute-start | bytes 786440 | tf_op jit(solution)/shard_map/ppermute | solution.py:59
  30.6 8.8 %collective-permute-start.2 = (bf16[128,1024]{1,0:T(8,128)(2,1)S(1)}, bf16[128,1024]{1,0:T(8,128)(2,1)S(1)}, u32[]{:S(2)}, u32[]{:S(2)}) collective-permute-start(bf16[128,1024]{1,0:T(8,128)(2,1)S(1)} %pad_maximum_fusion.1.refs_0_), channel_id=1, source_target_pairs={{0,16},{8,24},{16,32},{24,40},{32,48},{40,56},{48,64},{56,72},{64,... | collective-permute-start | bytes 786440 | tf_op jit(solution)/shard_map/ppermute | solution.py:58
  38.3 6.9 %collective-permute-start.5 = (bf16[128,1024]{1,0:T(8,128)(2,1)S(1)}, bf16[128,1024]{1,0:T(8,128)(2,1)S(1)}, u32[]{:S(2)}, u32[]{:S(2)}) collective-permute-start(bf16[128,1024]{1,0:T(8,128)(2,1)S(1)} %collective-permute-done.3.refs_2_), channel_id=1, source_target_pairs={{16,0},{24,8},{32,16},{40,24},{48,32},{56,40},{64,48},{72,56},{80,... | collective-permute-start | bytes 786440 | tf_op jit(solution)/shard_map/ppermute | solution.py:59
  39.4 9.2 %collective-permute-start.4 = (bf16[128,1024]{1,0:T(8,128)(2,1)S(1)}, bf16[128,1024]{1,0:T(8,128)(2,1)S(1)}, u32[]{:S(2)}, u32[]{:S(2)}) collective-permute-start(bf16[128,1024]{1,0:T(8,128)(2,1)S(1)} %collective-permute-done.2.refs_1_), channel_id=1, source_target_pairs={{0,16},{8,24},{16,32},{24,40},{32,48},{40,56},{48,64},{56,72},{64,... | collective-permute-start | bytes 786440 | tf_op jit(solution)/shard_map/ppermute | solution.py:58
  48.7 17.7 %copy-start.18 = (f32[2,2048]{1,0:T(2,128)S(1)}, f32[2,2048]{1,0:T(2,128)}, u32[]{:S(2)}) copy-start(f32[2,2048]{1,0:T(2,128)} %param.15) | copy-start | bytes 49156
  48.7 18.8 %collective-permute-start.6 = (bf16[5,128,1024]{2,1,0:T(8,128)(2,1)S(1)}, bf16[5,128,1024]{2,1,0:T(8,128)(2,1)}, u32[]{:S(2)}, u32[]{:S(2)}) collective-permute-start(bf16[5,128,1024]{2,1,0:T(8,128)(2,1)S(1)} %stack.6.refs_0_), channel_id=1, source_target_pairs={{0,8},{8,0},{16,24},{24,16},{32,40},{40,32},{48,56},{56,48},{64,72... | collective-permute-start | bytes 3932168 | tf_op jit(solution)/shard_map/ppermute | solution.py:37
  49.6 7.7 %collective-permute-start.8 = (bf16[128,1024]{1,0:T(8,128)(2,1)S(1)}, bf16[128,1024]{1,0:T(8,128)(2,1)S(1)}, u32[]{:S(2)}, u32[]{:S(2)}) collective-permute-start(bf16[128,1024]{1,0:T(8,128)(2,1)S(1)} %collective-permute-done.5.refs_4_), channel_id=1, source_target_pairs={{16,0},{24,8},{32,16},{40,24},{48,32},{56,40},{64,48},{72,56},{80,... | collective-permute-start | bytes 786440 | tf_op jit(solution)/shard_map/ppermute | solution.py:59
  49.6 9.3 %collective-permute-start.7 = (bf16[128,1024]{1,0:T(8,128)(2,1)S(1)}, bf16[128,1024]{1,0:T(8,128)(2,1)S(1)}, u32[]{:S(2)}, u32[]{:S(2)}) collective-permute-start(bf16[128,1024]{1,0:T(8,128)(2,1)S(1)} %collective-permute-done.4.refs_3_), channel_id=1, source_target_pairs={{0,16},{8,24},{16,32},{24,40},{32,48},{40,56},{48,64},{56,72},{64,... | collective-permute-start | bytes 786440 | tf_op jit(solution)/shard_map/ppermute | solution.py:58
  57.3 3.9 %collective-permute-start.11 = (bf16[64,1024]{1,0:T(8,128)(2,1)S(1)}, bf16[64,1024]{1,0:T(8,128)(2,1)S(1)}, u32[]{:S(2)}, u32[]{:S(2)}) collective-permute-start(bf16[64,1024]{1,0:T(8,128)(2,1)S(1)} %slice.65), channel_id=1, source_target_pairs={{16,0},{24,8},{32,16},{40,24},{48,32},{56,40},{64,48},{72,56},{80,... | collective-permute-start | bytes 393224 | tf_op jit(solution)/shard_map/ppermute | solution.py:59
  58.9 5.1 %collective-permute-start.10 = (bf16[64,1024]{1,0:T(8,128)(2,1)S(1)}, bf16[64,1024]{1,0:T(8,128)(2,1)S(1)}, u32[]{:S(2)}, u32[]{:S(2)}) collective-permute-start(bf16[64,1024]{1,0:T(8,128)(2,1)S(1)} %slice.64), channel_id=1, source_target_pairs={{0,16},{8,24},{16,32},{24,40},{32,48},{40,56},{48,64},{56,72},{64,... | collective-permute-start | bytes 393224 | tf_op jit(solution)/shard_map/ppermute | solution.py:58
  59.1 8.4 %collective-permute-start.9 = (bf16[2,128,1024]{2,1,0:T(8,128)(2,1)S(1)}, bf16[2,128,1024]{2,1,0:T(8,128)(2,1)}, u32[]{:S(2)}, u32[]{:S(2)}) collective-permute-start(bf16[2,128,1024]{2,1,0:T(8,128)(2,1)S(1)} %stack.7.refs_2_), channel_id=1, source_target_pairs={{0,8},{8,0},{16,24},{24,16},{32,40},{40,32},{48,56},{56,48},{64,72... | collective-permute-start | bytes 1572872 | tf_op jit(solution)/shard_map/ppermute | solution.py:37
  64.1 3.4 %collective-permute-start.12 = (bf16[2,64,1024]{2,1,0:T(8,128)(2,1)S(1)}, bf16[2,64,1024]{2,1,0:T(8,128)(2,1)S(1)}, u32[]{:S(2)}, u32[]{:S(2)}) collective-permute-start(bf16[2,64,1024]{2,1,0:T(8,128)(2,1)S(1)} %stack.8.refs_4_), channel_id=1, source_target_pairs={{0,8},{8,0},{16,24},{24,16},{32,40},{40,32},{48,56},{56,48},{64,72... | collective-permute-start | bytes 786440 | tf_op jit(solution)/shard_map/ppermute | solution.py:37
  67.5 2.3 %copy-start.2 = (bf16[2,64,1024]{2,1,0:T(8,128)(2,1)}, bf16[2,64,1024]{2,1,0:T(8,128)(2,1)S(1)}, u32[]{:S(2)}) copy-start(bf16[2,64,1024]{2,1,0:T(8,128)(2,1)S(1)} %collective-permute-done.12.refs_5_) | copy-start | bytes 786436
  67.5 4.5 %copy-start.17 = (f32[2,4,15,31]{3,1,2,0:T(4,128)S(1)}, f32[2,4,15,31]{3,1,2,0:T(4,128)}, u32[]{:S(2)}) copy-start(f32[2,4,15,31]{3,1,2,0:T(4,128)} %param.17) | copy-start | bytes 44644
  67.5 4.6 %copy-start.10 = (bf16[128,256]{1,0:T(8,128)(2,1)S(1)}, bf16[128,256]{1,0:T(8,128)(2,1)}, u32[]{:S(2)}) copy-start(bf16[128,256]{1,0:T(8,128)(2,1)} %get-tuple-element.55) | copy-start | bytes 196612
  67.6 4.6 %copy-start.11 = (bf16[128,256]{1,0:T(8,128)(2,1)S(1)}, bf16[128,256]{1,0:T(8,128)(2,1)}, u32[]{:S(2)}) copy-start(bf16[128,256]{1,0:T(8,128)(2,1)} %get-tuple-element.46) | copy-start | bytes 196612
  67.6 4.6 %copy-start.12 = (bf16[128,256]{1,0:T(8,128)(2,1)S(1)}, bf16[128,256]{1,0:T(8,128)(2,1)}, u32[]{:S(2)}) copy-start(bf16[128,256]{1,0:T(8,128)(2,1)} %get-tuple-element.57) | copy-start | bytes 196612
  67.6 4.6 %copy-start.9 = (s32[256]{0:T(256)S(1)}, s32[256]{0:T(256)}, u32[]{:S(2)}) copy-start(s32[256]{0:T(256)} %param.10) | copy-start | bytes 3076
  69.8 9.2 %collective-permute-start.14 = (bf16[256,512]{1,0:T(8,128)(2,1)S(1)}, bf16[256,512]{1,0:T(8,128)(2,1)S(1)}, u32[]{:S(2)}, u32[]{:S(2)}) collective-permute-start(bf16[256,512]{1,0:T(8,128)(2,1)S(1)} %project.5.own_ref), channel_id=1, source_target_pairs={{8,16},{24,32},{40,48},{56,64},{72,80},{88,96},{104,112},{16,8},{3... | collective-permute-start | bytes 786440 | tf_op jit(solution)/shard_map/ppermute | solution.py:43
  71.8 7.2 %collective-permute-start.13 = (bf16[256,512]{1,0:T(8,128)(2,1)S(1)}, bf16[256,512]{1,0:T(8,128)(2,1)S(1)}, u32[]{:S(2)}, u32[]{:S(2)}) collective-permute-start(bf16[256,512]{1,0:T(8,128)(2,1)S(1)} %project.5.own_ref), channel_id=1, source_target_pairs={{0,8},{8,0},{16,24},{24,16},{32,40},{40,32},{48,56},{56,48},{64,72... | collective-permute-start | bytes 786440 | tf_op jit(solution)/shard_map/ppermute | solution.py:37
  74.6 1.6 copy-start
  76.2 0.9 copy-start.3
  82.1 35.9 %all-to-all-start.1 = ((bf16[8,256,256]{2,1,0:T(8,128)(2,1)}), bf16[8,256,256]{2,1,0:T(8,128)(2,1)S(1)}, u32[]{:S(2)}, u32[]{:S(2)}) async-start(bf16[8,256,256]{2,1,0:T(8,128)(2,1)} %attend.2), calls=%async_computation.1 | async-start | bytes 2097152 | tf_op jit(solution)/shard_map/all_to_all | solution.py:32
  88.8 7.8 %collective-permute-start.17 = (bf16[128,1024]{1,0:T(8,128)(2,1)S(1)}, bf16[128,1024]{1,0:T(8,128)(2,1)S(1)}, u32[]{:S(2)}, u32[]{:S(2)}) collective-permute-start(bf16[128,1024]{1,0:T(8,128)(2,1)S(1)} %pad_maximum_fusion.refs_0_), channel_id=1, source_target_pairs={{16,0},{24,8},{32,16},{40,24},{48,32},{56,40},{64,48},{72,56},{80,... | collective-permute-start | bytes 786440 | tf_op jit(solution)/shard_map/ppermute | solution.py:59
  89.0 8.7 %collective-permute-start.15 = (bf16[128,1024]{1,0:T(8,128)(2,1)S(1)}, bf16[128,1024]{1,0:T(8,128)(2,1)S(1)}, u32[]{:S(2)}, u32[]{:S(2)}) collective-permute-start(bf16[128,1024]{1,0:T(8,128)(2,1)S(1)} %pad_maximum_fusion.refs_0_), channel_id=1, source_target_pairs={{0,16},{8,24},{16,32},{24,40},{32,48},{40,56},{48,64},{56,72},{64,... | collective-permute-start | bytes 786440 | tf_op jit(solution)/shard_map/ppermute | solution.py:58
  96.7 6.7 %collective-permute-start.18 = (bf16[128,1024]{1,0:T(8,128)(2,1)S(1)}, bf16[128,1024]{1,0:T(8,128)(2,1)S(1)}, u32[]{:S(2)}, u32[]{:S(2)}) collective-permute-start(bf16[128,1024]{1,0:T(8,128)(2,1)S(1)} %collective-permute-done.17.refs_2_), channel_id=1, source_target_pairs={{16,0},{24,8},{32,16},{40,24},{48,32},{56,40},{64,48},{72,56},{80,... | collective-permute-start | bytes 786440 | tf_op jit(solution)/shard_map/ppermute | solution.py:59
  97.7 22.0 %copy-start.4 = (bf16[128,1024]{1,0:T(8,128)(2,1)}, bf16[128,1024]{1,0:T(8,128)(2,1)S(1)}, u32[]{:S(2)}) copy-start(bf16[128,1024]{1,0:T(8,128)(2,1)S(1)} %collective-permute-done.15.refs_1_) | copy-start | bytes 786436
  97.7 7.6 %collective-permute-start.16 = (bf16[128,1024]{1,0:T(8,128)(2,1)S(1)}, bf16[128,1024]{1,0:T(8,128)(2,1)S(1)}, u32[]{:S(2)}, u32[]{:S(2)}) collective-permute-start(bf16[128,1024]{1,0:T(8,128)(2,1)S(1)} %collective-permute-done.15.refs_1_), channel_id=1, source_target_pairs={{0,16},{8,24},{16,32},{24,40},{32,48},{40,56},{48,64},{56,72},{64,... | collective-permute-start | bytes 786440 | tf_op jit(solution)/shard_map/ppermute | solution.py:58
  119.7 33.5 %all-to-all-start.2 = ((bf16[8,256,256]{2,1,0:T(8,128)(2,1)}), bf16[8,256,256]{2,1,0:T(8,128)(2,1)}, u32[]{:S(2)}, u32[]{:S(2)}) async-start(bf16[8,256,256]{2,1,0:T(8,128)(2,1)} %summed.1), calls=%async_computation.2 | async-start | bytes 2097152 | tf_op jit(solution)/shard_map/all_to_all | solution.py:32
  124.2 1.0 copy-start.5
  125.2 31.3 %collective-permute-start.19 = (bf16[5,128,1024]{2,1,0:T(8,128)(2,1)S(1)}, bf16[5,128,1024]{2,1,0:T(8,128)(2,1)}, u32[]{:S(2)}, u32[]{:S(2)}) collective-permute-start(bf16[5,128,1024]{2,1,0:T(8,128)(2,1)S(1)} %stack.9.refs_0_), channel_id=1, source_target_pairs={{0,8},{8,0},{16,24},{24,16},{32,40},{40,32},{48,56},{56,48},{64,72... | collective-permute-start | bytes 3932168 | tf_op jit(solution)/shard_map/ppermute | solution.py:37
  125.8 8.5 %collective-permute-start.21 = (bf16[128,1024]{1,0:T(8,128)(2,1)S(1)}, bf16[128,1024]{1,0:T(8,128)(2,1)S(1)}, u32[]{:S(2)}, u32[]{:S(2)}) collective-permute-start(bf16[128,1024]{1,0:T(8,128)(2,1)S(1)} %collective-permute-done.18.refs_4_), channel_id=1, source_target_pairs={{16,0},{24,8},{32,16},{40,24},{48,32},{56,40},{64,48},{72,56},{80,... | collective-permute-start | bytes 786440 | tf_op jit(solution)/shard_map/ppermute | solution.py:59
  126.0 8.8 %collective-permute-start.20 = (bf16[128,1024]{1,0:T(8,128)(2,1)S(1)}, bf16[128,1024]{1,0:T(8,128)(2,1)S(1)}, u32[]{:S(2)}, u32[]{:S(2)}) collective-permute-start(bf16[128,1024]{1,0:T(8,128)(2,1)S(1)} %collective-permute-done.16.refs_3_), channel_id=1, source_target_pairs={{0,16},{8,24},{16,32},{24,40},{32,48},{40,56},{48,64},{56,72},{64,... | collective-permute-start | bytes 786440 | tf_op jit(solution)/shard_map/ppermute | solution.py:58
  134.8 21.7 %collective-permute-start.22 = (bf16[2,128,1024]{2,1,0:T(8,128)(2,1)S(1)}, bf16[2,128,1024]{2,1,0:T(8,128)(2,1)}, u32[]{:S(2)}, u32[]{:S(2)}) collective-permute-start(bf16[2,128,1024]{2,1,0:T(8,128)(2,1)S(1)} %stack.10.refs_2_), channel_id=1, source_target_pairs={{0,8},{8,0},{16,24},{24,16},{32,40},{40,32},{48,56},{56,48},{64,72... | collective-permute-start | bytes 1572872 | tf_op jit(solution)/shard_map/ppermute | solution.py:37
  136.1 5.2 %collective-permute-start.24 = (bf16[64,1024]{1,0:T(8,128)(2,1)S(1)}, bf16[64,1024]{1,0:T(8,128)(2,1)S(1)}, u32[]{:S(2)}, u32[]{:S(2)}) collective-permute-start(bf16[64,1024]{1,0:T(8,128)(2,1)S(1)} %slice.67), channel_id=1, source_target_pairs={{16,0},{24,8},{32,16},{40,24},{48,32},{56,40},{64,48},{72,56},{80,... | collective-permute-start | bytes 393224 | tf_op jit(solution)/shard_map/ppermute | solution.py:59
  136.4 6.2 %collective-permute-start.23 = (bf16[64,1024]{1,0:T(8,128)(2,1)S(1)}, bf16[64,1024]{1,0:T(8,128)(2,1)S(1)}, u32[]{:S(2)}, u32[]{:S(2)}) collective-permute-start(bf16[64,1024]{1,0:T(8,128)(2,1)S(1)} %slice.66), channel_id=1, source_target_pairs={{0,16},{8,24},{16,32},{24,40},{32,48},{40,56},{48,64},{56,72},{64,... | collective-permute-start | bytes 393224 | tf_op jit(solution)/shard_map/ppermute | solution.py:58
  142.6 13.9 %collective-permute-start.25 = (bf16[2,64,1024]{2,1,0:T(8,128)(2,1)S(1)}, bf16[2,64,1024]{2,1,0:T(8,128)(2,1)S(1)}, u32[]{:S(2)}, u32[]{:S(2)}) collective-permute-start(bf16[2,64,1024]{2,1,0:T(8,128)(2,1)S(1)} %stack.11.refs_4_), channel_id=1, source_target_pairs={{0,8},{8,0},{16,24},{24,16},{32,40},{40,32},{48,56},{56,48},{64,72... | collective-permute-start | bytes 786440 | tf_op jit(solution)/shard_map/ppermute | solution.py:37
  158.5 8.2 %collective-permute-start.27 = (bf16[256,512]{1,0:T(8,128)(2,1)S(1)}, bf16[256,512]{1,0:T(8,128)(2,1)S(1)}, u32[]{:S(2)}, u32[]{:S(2)}) collective-permute-start(bf16[256,512]{1,0:T(8,128)(2,1)S(1)} %project.7.own_ref), channel_id=1, source_target_pairs={{8,16},{24,32},{40,48},{56,64},{72,80},{88,96},{104,112},{16,8},{3... | collective-permute-start | bytes 786440 | tf_op jit(solution)/shard_map/ppermute | solution.py:43
  162.7 4.0 %collective-permute-start.26 = (bf16[256,512]{1,0:T(8,128)(2,1)S(1)}, bf16[256,512]{1,0:T(8,128)(2,1)S(1)}, u32[]{:S(2)}, u32[]{:S(2)}) collective-permute-start(bf16[256,512]{1,0:T(8,128)(2,1)S(1)} %project.7.own_ref), channel_id=1, source_target_pairs={{0,8},{8,0},{16,24},{24,16},{32,40},{40,32},{48,56},{56,48},{64,72... | collective-permute-start | bytes 786440 | tf_op jit(solution)/shard_map/ppermute | solution.py:37
  162.9 3.9 %copy-start.1 = (f32[4,256,768]{2,1,0:T(8,128)S(1)}, f32[4,256,768]{2,1,0:T(8,128)}, u32[]{:S(2)}) copy-start(f32[4,256,768]{2,1,0:T(8,128)} %copy-done) | copy-start | bytes 9437188
  199.6 9.3 %copy-start.7 = (bf16[256,256]{1,0:T(8,128)(2,1)S(1)}, bf16[256,256]{1,0:T(8,128)(2,1)}, u32[]{:S(2)}) copy-start(bf16[256,256]{1,0:T(8,128)(2,1)} %copy-done.6) | copy-start | bytes 393220
  (2 other events, 1.6 us)

commit v3 on v2

--- a/solution.py
+++ b/solution.py
@@ -427,14 +427,15 @@
 ):
     tokens, width = stream.shape
 
-    def side_by_side(layer):
-        mats = (k_weight, v_weight, q_weight, out_weight)
+    mats = (k_weight, v_weight, q_weight, out_weight)
+
+    def side_by_side(layer, mats):
         return jnp.concatenate([m[layer] for m in mats], axis=1)
 
     doc_near, doc_far = partner(documents), across(documents)
     x_copies = spread(stream, post_gain[0], lax.axis_size("tp"))
     x_all = exchange(x_copies, "tp")
-    chunk, doc_near, doc_far = lax.optimization_barrier((side_by_side(0), doc_near, doc_far))
+    chunk, doc_near, doc_far = lax.optimization_barrier((side_by_side(0, mats), doc_near, doc_far))
     biases = prepare(documents, doc_near, doc_far, offset_bias)
     slots = ring(chunk)
     weights = with_partner(slots)
@@ -449,9 +450,10 @@
         return attend(queries, kv, near, far, biases[layer], w_out)
 
     scaled, inverse = scale(x_all, None, pre_gain[0], tokens)
+    inverse, mats = lax.optimization_barrier((inverse, mats))
     partial_sums = block(0, scaled, inverse, weights)
     chunk, partial_sums = lax.optimization_barrier(
-        (side_by_side(1), partial_sums)
+        (side_by_side(1, mats), partial_sums)
     )
     slots = ring(chunk)
     arrived = exchange(partial_sums, "tp")

time: 210 us -> 210 us (level)
    all_to_all x3, waiting for transfers between devices: 22.1 us -> 18 us  [exchange(): return lax.all_to_all(x, axis, split_axis=0, concat_axis=0, tiled=True)]
    ppermute x3, waiting for transfers between devices: 1.94 us -> 5.29 us  [across(): return lax.ppermute(x, 'sp', moves + [(j, i) for i, j in moves])]
    unnamed x39 -> x41, local copies, waits for them, and re-layouts: 5.13 us -> 5.88 us
  transfers between devices with their start and end apart: 31 -> 31, of which waited for: 18 -> 18; matrix products, arithmetic and copies ran while one was open for 1% -> 0% of each run, Pallas kernels for 5% -> 5%
where the time goes in v3:
time: 210 us; the launch traced here: 209 us
  waiting for transfers between devices  74.1 us (35%)
  starting transfers between devices  65.5 us (31%)
  blocking collectives  39.7 us (19%)
  Pallas kernels  21.7 us (10%)
  local copies, waits for them, and re-layouts  6.75 us (3%)
    ppermute x8, waiting for transfers between devices, ring(): right = lax.ppermute(right, 'sp', down)  40.8 us
    all_to_all x2, blocking collectives, exchange(): return lax.all_to_all(x, axis, split_axis=0, concat_axis=0, tiled=True)  39.7 us
    ppermute x9, starting transfers between devices, partner(): return lax.ppermute(x, 'sp', [(i, i ^ 1) for i in range(count)])  28.7 us
    all_to_all x3, waiting for transfers between devices, exchange(): return lax.all_to_all(x, axis, split_axis=0, concat_axis=0, tiled=True)  18 us
    all_to_all x3, starting transfers between devices, exchange(): return lax.all_to_all(x, axis, split_axis=0, concat_axis=0, tiled=True)  15 us
    ppermute x8, waiting for transfers between devices, ring(): left = lax.ppermute(left, 'sp', up)  10.1 us
    ppermute x3, starting transfers between devices, across(): return lax.ppermute(x, 'sp', moves + [(j, i) for i, j in moves])  9.44 us
    pallas_call x4, Pallas kernels, project(): pl.pallas_call(functools.partial(project_kernel, weight_places(weights),...  8.03 us
  transfers between devices with their start and end apart: 31, of which 18 were waited for; matrix products, arithmetic and copies ran while one was open for 0% of the time, Pallas kernels for 5%

profile of v3, /device:TPU:513, one launch (start us, length us, event | category | flops | bytes accessed | tf_op | source)
XLA Modules:
  0.0 209.4 jit_solution(11130276476351054589)
XLA Ops:
  0.0 20.4 %collective-permute-start = (s32[256]{0:T(256)}, s32[256]{0:T(256)S(1)}, u32[]{:S(2)}, u32[]{:S(2)}) collective-permute-start(s32[256]{0:T(256)} %param.10), channel_id=1, source_target_pairs={{0,8},{8,0},{16,24},{24,16},{32,40},{40,32},{48,56},{56,48},{64,72... | collective-permute-start | bytes 3080 | tf_op jit(solution)/shard_map/ppermute | solution.py:37
  20.4 1.9 collective-permute-start.1
  24.0 1.2 spread.1
  25.2 3.9 %all-to-all-start = ((bf16[8,264,256]{2,1,0:T(8,128)(2,1)}), bf16[8,264,256]{2,1,0:T(8,128)(2,1)S(1)}, u32[]{:S(2)}, u32[]{:S(2)}) async-start(bf16[8,264,256]{2,1,0:T(8,128)(2,1)} %spread.1), calls=%async_computation | async-start | bytes 2162688 | tf_op jit(solution)/shard_map/all_to_all | solution.py:32
  29.4 1.4 collective-permute-start.2
  30.8 6.3 %collective-permute-done.3.refs_2_ = bf16[128,1024]{1,0:T(8,128)(2,1)S(1)} collective-permute-done((bf16[128,1024]{1,0:T(8,128)(2,1)S(1)}, bf16[128,1024]{1,0:T(8,128)(2,1)S(1)}, u32[]{:S(2)}, u32[]{:S(2)}) %collective-permute-start.3) | collective-permute-done | bytes 262176 | tf_op jit(solution)/shard_map/ppermute | solution.py:59
  38.6 5.4 %collective-permute-done.5.refs_4_ = bf16[128,1024]{1,0:T(8,128)(2,1)S(1)} collective-permute-done((bf16[128,1024]{1,0:T(8,128)(2,1)S(1)}, bf16[128,1024]{1,0:T(8,128)(2,1)S(1)}, u32[]{:S(2)}, u32[]{:S(2)}) %collective-permute-start.5) | collective-permute-done | bytes 262176 | tf_op jit(solution)/shard_map/ppermute | solution.py:59
  44.0 3.4 %collective-permute-done.4.refs_3_ = bf16[128,1024]{1,0:T(8,128)(2,1)S(1)} collective-permute-done((bf16[128,1024]{1,0:T(8,128)(2,1)S(1)}, bf16[128,1024]{1,0:T(8,128)(2,1)S(1)}, u32[]{:S(2)}, u32[]{:S(2)}) %collective-permute-start.4) | collective-permute-done | bytes 262176 | tf_op jit(solution)/shard_map/ppermute | solution.py:58
  48.4 1.5 collective-permute-start.7
  49.9 6.3 %collective-permute-done.8.refs_1_ = bf16[128,1024]{1,0:T(8,128)(2,1)S(1)} collective-permute-done((bf16[128,1024]{1,0:T(8,128)(2,1)S(1)}, bf16[128,1024]{1,0:T(8,128)(2,1)S(1)}, u32[]{:S(2)}, u32[]{:S(2)}) %collective-permute-start.8) | collective-permute-done | bytes 262176 | tf_op jit(solution)/shard_map/ppermute | solution.py:59
  56.1 1.6 collective-permute-start.11
  57.9 1.6 collective-permute-start.9
  60.1 2.8 %collective-permute-done.10.refs_0_ = bf16[64,1024]{1,0:T(8,128)(2,1)S(1)} collective-permute-done((bf16[64,1024]{1,0:T(8,128)(2,1)S(1)}, bf16[64,1024]{1,0:T(8,128)(2,1)S(1)}, u32[]{:S(2)}, u32[]{:S(2)}) %collective-permute-start.10) | collective-permute-done | bytes 131104 | tf_op jit(solution)/shard_map/ppermute | solution.py:58
  62.9 2.3 %collective-permute-start.12 = (bf16[2,64,1024]{2,1,0:T(8,128)(2,1)S(1)}, bf16[2,64,1024]{2,1,0:T(8,128)(2,1)S(1)}, u32[]{:S(2)}, u32[]{:S(2)}) collective-permute-start(bf16[2,64,1024]{2,1,0:T(8,128)(2,1)S(1)} %stack.8.refs_4_), channel_id=1, source_target_pairs={{0,8},{8,0},{16,24},{24,16},{32,40},{40,32},{48,56},{56,48},{64,72... | collective-permute-start | bytes 786440 | tf_op jit(solution)/shard_map/ppermute | solution.py:37
  65.2 2.4 %prepare.1 = (f32[4,256,768]{2,1,0:T(8,128)S(1)}, f32[4,256,768]{2,1,0:T(8,128)S(1)}) custom-call(s32[1,256]{1,0:T(1,128)S(1)} %bitcast.24, s32[1,256]{1,0:T(1,128)S(1)} %bitcast.25, s32[1,256]{1,0:T(1,128)S(1)} %bitcast.26, f32[2,4,15,128]{3,2,1,0:T(8,128)S(1)} %pad.4.table_ref), custom_call_target="tpu_custom_call" | custom-call | flops 6291456 | bytes 6291456 | tf_op jit(solution)/shard_map/prepare/pallas_call | solution.py:185
  67.6 1.6 copy-done
  69.3 1.7 copy-done.2
  71.4 2.1 %project.5.own_ref = bf16[256,512]{1,0:T(8,128)(2,1)S(1)} custom-call(bf16[256,2048]{1,0:T(8,128)(2,1)S(1)} %get-tuple-element.34.scaled_ref, f32[256,1]{1,0:T(8,128)S(1)} %get-tuple-element.35.inverse_ref, bf16[5,128,1024]{2,1,0:T(8,128)(2,1)S(1)} %stack.6.refs_0_, bf16[5,128,1024]{2,1,0:T(8,128)(2,1)} %collective-permute-done.6.refs_1_, ...), custom_call_target="tpu_custom_call" | custom-call | flops 536870912 | bytes 4194304 | tf_op jit(solution)/shard_map/project/pallas_call | solution.py:276
  73.5 2.0 collective-permute-start.14
  75.9 1.9 project.4
  77.9 3.4 %collective-permute-done.14.far_ref = bf16[256,512]{1,0:T(8,128)(2,1)S(1)} collective-permute-done((bf16[256,512]{1,0:T(8,128)(2,1)S(1)}, bf16[256,512]{1,0:T(8,128)(2,1)S(1)}, u32[]{:S(2)}, u32[]{:S(2)}) %collective-permute-start.14) | collective-permute-done | bytes 262176 | tf_op jit(solution)/shard_map/ppermute | solution.py:43
  81.2 3.1 %attend.2 = bf16[8,256,256]{2,1,0:T(8,128)(2,1)} custom-call(bf16[256,256]{1,0:T(8,128)(2,1)S(1)} %get-tuple-element.37.q_ref, bf16[256,512]{1,0:T(8,128)(2,1)S(1)} %project.5.own_ref, bf16[256,512]{1,0:T(8,128)(2,1)S(1)} %collective-permute-done.13.near_ref, bf16[256,512]{1,0:T(8,128)(2,1)S(1)} %collective-permute-done.14.far_ref, ...), custom_call_target="tpu_custom_call" | custom-call | flops 671088640 | bytes 4194304 | tf_op jit(solution)/shard_map/attend/pallas_call | solution.py:354
  84.4 6.7 %all-to-all-start.1 = ((bf16[8,256,256]{2,1,0:T(8,128)(2,1)}), bf16[8,256,256]{2,1,0:T(8,128)(2,1)S(1)}, u32[]{:S(2)}, u32[]{:S(2)}) async-start(bf16[8,256,256]{2,1,0:T(8,128)(2,1)} %attend.2), calls=%async_computation.1 | async-start | bytes 2097152 | tf_op jit(solution)/shard_map/all_to_all | solution.py:32
  91.1 1.4 collective-permute-start.15
  92.5 6.0 %collective-permute-done.17.refs_2_ = bf16[128,1024]{1,0:T(8,128)(2,1)S(1)} collective-permute-done((bf16[128,1024]{1,0:T(8,128)(2,1)S(1)}, bf16[128,1024]{1,0:T(8,128)(2,1)S(1)}, u32[]{:S(2)}, u32[]{:S(2)}) %collective-permute-start.17) | collective-permute-done | bytes 262176 | tf_op jit(solution)/shard_map/ppermute | solution.py:59
  98.5 1.5 collective-permute-start.18
  100.4 6.4 %collective-permute-done.18.refs_4_ = bf16[128,1024]{1,0:T(8,128)(2,1)S(1)} collective-permute-done((bf16[128,1024]{1,0:T(8,128)(2,1)S(1)}, bf16[128,1024]{1,0:T(8,128)(2,1)S(1)}, u32[]{:S(2)}, u32[]{:S(2)}) %collective-permute-start.18) | collective-permute-done | bytes 262176 | tf_op jit(solution)/shard_map/ppermute | solution.py:59
  106.8 1.0 collective-permute-done.16.refs_3_
  107.9 10.5 %all-to-all-done.1.arrived_ref = bf16[8,256,256]{2,1,0:T(8,128)(2,1)S(1)} async-done(((bf16[8,256,256]{2,1,0:T(8,128)(2,1)}), bf16[8,256,256]{2,1,0:T(8,128)(2,1)S(1)}, u32[]{:S(2)}, u32[]{:S(2)}) %all-to-all-start.1) | async-done | bytes 1048608 | tf_op jit(solution)/shard_map/all_to_all | solution.py:32
  118.4 1.7 summed.1
  120.1 4.4 %all-to-all-start.2 = ((bf16[8,256,256]{2,1,0:T(8,128)(2,1)}), bf16[8,256,256]{2,1,0:T(8,128)(2,1)}, u32[]{:S(2)}, u32[]{:S(2)}) async-start(bf16[8,256,256]{2,1,0:T(8,128)(2,1)} %summed.1), calls=%async_computation.2 | async-start | bytes 2097152 | tf_op jit(solution)/shard_map/all_to_all | solution.py:32
  126.1 1.5 collective-permute-start.20
  127.5 6.4 %collective-permute-done.21.refs_1_ = bf16[128,1024]{1,0:T(8,128)(2,1)S(1)} collective-permute-done((bf16[128,1024]{1,0:T(8,128)(2,1)S(1)}, bf16[128,1024]{1,0:T(8,128)(2,1)S(1)}, u32[]{:S(2)}, u32[]{:S(2)}) %collective-permute-start.21) | collective-permute-done | bytes 262176 | tf_op jit(solution)/shard_map/ppermute | solution.py:59
  133.9 1.1 collective-permute-done.20.refs_0_
  135.0 1.2 collective-permute-start.22
  136.6 1.3 collective-permute-start.23
  137.9 3.5 %collective-permute-done.24.refs_1_ = bf16[64,1024]{1,0:T(8,128)(2,1)S(1)} collective-permute-done((bf16[64,1024]{1,0:T(8,128)(2,1)S(1)}, bf16[64,1024]{1,0:T(8,128)(2,1)S(1)}, u32[]{:S(2)}, u32[]{:S(2)}) %collective-permute-start.24) | collective-permute-done | bytes 131104 | tf_op jit(solution)/shard_map/ppermute | solution.py:59
  141.4 1.3 collective-permute-done.23.refs_0_
  142.8 1.4 collective-permute-start.25
  144.2 7.4 %all-to-all-done.2.refs_1_ = bf16[8,256,256]{2,1,0:T(8,128)(2,1)} async-done(((bf16[8,256,256]{2,1,0:T(8,128)(2,1)}), bf16[8,256,256]{2,1,0:T(8,128)(2,1)}, u32[]{:S(2)}, u32[]{:S(2)}) %all-to-all-start.2) | async-done | bytes 1048608 | tf_op jit(solution)/shard_map/all_to_all | solution.py:32
  151.6 2.5 %scale.3 = (bf16[256,2048]{1,0:T(8,128)(2,1)S(1)}, f32[256,1]{1,0:T(8,128)S(1)}, bf16[256,256]{1,0:T(8,128)(2,1)S(1)}) custom-call(bf16[8,264,256]{2,1,0:T(8,128)(2,1)S(1)} %all-to-all-done.refs_0_, bf16[8,256,256]{2,1,0:T(8,128)(2,1)} %all-to-all-done.2.refs_1_, f32[8,1,256]{2,1,0:T(1,128)S(1)} %bitcast.22), custom_call_target="tpu_custom_call" | custom-call | flops 4194304 | bytes 4194304 | tf_op jit(solution)/shard_map/scale/pallas_call | solution.py:240
  154.8 2.0 project.7.own_ref
  156.9 5.5 %collective-permute-start.27 = (bf16[256,512]{1,0:T(8,128)(2,1)S(1)}, bf16[256,512]{1,0:T(8,128)(2,1)S(1)}, u32[]{:S(2)}, u32[]{:S(2)}) collective-permute-start(bf16[256,512]{1,0:T(8,128)(2,1)S(1)} %project.7.own_ref), channel_id=1, source_target_pairs={{8,16},{24,32},{40,48},{56,64},{72,80},{88,96},{104,112},{16,8},{3... | collective-permute-start | bytes 786440 | tf_op jit(solution)/shard_map/ppermute | solution.py:43
  162.6 1.9 project.6
  164.5 1.9 collective-permute-done.27.far_ref
  166.5 2.2 %attend.3 = bf16[8,256,256]{2,1,0:T(8,128)(2,1)S(1)} custom-call(bf16[256,256]{1,0:T(8,128)(2,1)S(1)} %get-tuple-element.50.q_ref, bf16[256,512]{1,0:T(8,128)(2,1)S(1)} %project.7.own_ref, bf16[256,512]{1,0:T(8,128)(2,1)S(1)} %collective-permute-done.26.near_ref, bf16[256,512]{1,0:T(8,128)(2,1)S(1)} %collective-permute-done.27.far_ref, ...), custom_call_target="tpu_custom_call" | custom-call | flops 671088640 | bytes 4194304 | tf_op jit(solution)/shard_map/attend/pallas_call | solution.py:354
  168.6 30.6 %all_to_all.25 = bf16[8,256,256]{2,1,0:T(8,128)(2,1)S(1)} all-to-all(bf16[8,256,256]{2,1,0:T(8,128)(2,1)S(1)} %attend.3), channel_id=1, replica_groups=mesh['grp'=2,'sp'=16,'tp'=8] {'tp'}, dimensions={0} | all-to-all | bytes 2097152 | tf_op jit(solution)/shard_map/all_to_all | solution.py:32
  199.6 9.0 %all_to_all.26 = f32[8,256,1]{1,2,0:T(1,128)S(1)} all-to-all(f32[8,256,1]{1,2,0:T(1,128)S(1)} %broadcast_in_dim.4), channel_id=1, replica_groups=mesh['grp'=2,'sp'=16,'tp'=8] {'tp'}, dimensions={0} | all-to-all | bytes 16384 | tf_op jit(solution)/shard_map/all_to_all | solution.py:32
  (93 shorter events, 10.0 us)
Async XLA Ops:
  0.0 29.2 %collective-permute-start = (s32[256]{0:T(256)}, s32[256]{0:T(256)S(1)}, u32[]{:S(2)}, u32[]{:S(2)}) collective-permute-start(s32[256]{0:T(256)} %param.10), channel_id=1, source_target_pairs={{0,8},{8,0},{16,24},{24,16},{32,40},{40,32},{48,56},{56,48},{64,72... | collective-permute-start | bytes 3080 | tf_op jit(solution)/shard_map/ppermute | solution.py:37
  20.4 8.8 %collective-permute-start.1 = (s32[256]{0:T(256)}, s32[256]{0:T(256)S(1)}, u32[]{:S(2)}, u32[]{:S(2)}) collective-permute-start(s32[256]{0:T(256)} %param.10), channel_id=1, source_target_pairs={{8,16},{24,32},{40,48},{56,64},{72,80},{88,96},{104,112},{16,8},{3... | collective-permute-start | bytes 3080 | tf_op jit(solution)/shard_map/ppermute | solution.py:43
  25.2 3.9 %copy-start.14 = (bf16[2,128,256]{2,1,0:T(8,128)(2,1)S(1)}, bf16[2,128,256]{2,1,0:T(8,128)(2,1)}, u32[]{:S(2)}) copy-start(bf16[2,128,256]{2,1,0:T(8,128)(2,1)} %param.14) | copy-start | bytes 393220
  25.2 3.9 %copy-start.16 = (bf16[2,128,256]{2,1,0:T(8,128)(2,1)S(1)}, bf16[2,128,256]{2,1,0:T(8,128)(2,1)}, u32[]{:S(2)}) copy-start(bf16[2,128,256]{2,1,0:T(8,128)(2,1)} %param.11) | copy-start | bytes 393220
  25.2 4.0 %copy-start.10 = (bf16[2,128,256]{2,1,0:T(8,128)(2,1)S(1)}, bf16[2,128,256]{2,1,0:T(8,128)(2,1)}, u32[]{:S(2)}) copy-start(bf16[2,128,256]{2,1,0:T(8,128)(2,1)} %param.13) | copy-start | bytes 393220
  25.2 4.0 %copy-start.12 = (bf16[2,128,256]{2,1,0:T(8,128)(2,1)S(1)}, bf16[2,128,256]{2,1,0:T(8,128)(2,1)}, u32[]{:S(2)}) copy-start(bf16[2,128,256]{2,1,0:T(8,128)(2,1)} %param.12) | copy-start | bytes 393220
  25.2 45.7 %all-to-all-start = ((bf16[8,264,256]{2,1,0:T(8,128)(2,1)}), bf16[8,264,256]{2,1,0:T(8,128)(2,1)S(1)}, u32[]{:S(2)}, u32[]{:S(2)}) async-start(bf16[8,264,256]{2,1,0:T(8,128)(2,1)} %spread.1), calls=%async_computation | async-start | bytes 2162688 | tf_op jit(solution)/shard_map/all_to_all | solution.py:32
  29.2 7.9 %collective-permute-start.3 = (bf16[128,1024]{1,0:T(8,128)(2,1)S(1)}, bf16[128,1024]{1,0:T(8,128)(2,1)S(1)}, u32[]{:S(2)}, u32[]{:S(2)}) collective-permute-start(bf16[128,1024]{1,0:T(8,128)(2,1)S(1)} %pad_maximum_fusion.1.refs_0_), channel_id=1, source_target_pairs={{16,0},{24,8},{32,16},{40,24},{48,32},{56,40},{64,48},{72,56},{80,... | collective-permute-start | bytes 786440 | tf_op jit(solution)/shard_map/ppermute | solution.py:59
  29.4 8.8 %collective-permute-start.2 = (bf16[128,1024]{1,0:T(8,128)(2,1)S(1)}, bf16[128,1024]{1,0:T(8,128)(2,1)S(1)}, u32[]{:S(2)}, u32[]{:S(2)}) collective-permute-start(bf16[128,1024]{1,0:T(8,128)(2,1)S(1)} %pad_maximum_fusion.1.refs_0_), channel_id=1, source_target_pairs={{0,16},{8,24},{16,32},{24,40},{32,48},{40,56},{48,64},{56,72},{64,... | collective-permute-start | bytes 786440 | tf_op jit(solution)/shard_map/ppermute | solution.py:58
  37.1 6.9 %collective-permute-start.5 = (bf16[128,1024]{1,0:T(8,128)(2,1)S(1)}, bf16[128,1024]{1,0:T(8,128)(2,1)S(1)}, u32[]{:S(2)}, u32[]{:S(2)}) collective-permute-start(bf16[128,1024]{1,0:T(8,128)(2,1)S(1)} %collective-permute-done.3.refs_2_), channel_id=1, source_target_pairs={{16,0},{24,8},{32,16},{40,24},{48,32},{56,40},{64,48},{72,56},{80,... | collective-permute-start | bytes 786440 | tf_op jit(solution)/shard_map/ppermute | solution.py:59
  38.2 9.2 %collective-permute-start.4 = (bf16[128,1024]{1,0:T(8,128)(2,1)S(1)}, bf16[128,1024]{1,0:T(8,128)(2,1)S(1)}, u32[]{:S(2)}, u32[]{:S(2)}) collective-permute-start(bf16[128,1024]{1,0:T(8,128)(2,1)S(1)} %collective-permute-done.2.refs_1_), channel_id=1, source_target_pairs={{0,16},{8,24},{16,32},{24,40},{32,48},{40,56},{48,64},{56,72},{64,... | collective-permute-start | bytes 786440 | tf_op jit(solution)/shard_map/ppermute | solution.py:58
  47.5 12.1 %copy-start.18 = (f32[2,4,15,31]{3,1,2,0:T(4,128)S(1)}, f32[2,4,15,31]{3,1,2,0:T(4,128)}, u32[]{:S(2)}) copy-start(f32[2,4,15,31]{3,1,2,0:T(4,128)} %param.17) | copy-start | bytes 44644
  47.5 17.7 %copy-start.19 = (f32[2,2048]{1,0:T(2,128)S(1)}, f32[2,2048]{1,0:T(2,128)}, u32[]{:S(2)}) copy-start(f32[2,2048]{1,0:T(2,128)} %param.15) | copy-start | bytes 49156
  47.5 17.7 %copy-start.9 = (s32[256]{0:T(256)S(1)}, s32[256]{0:T(256)}, u32[]{:S(2)}) copy-start(s32[256]{0:T(256)} %param.10) | copy-start | bytes 3076
  47.5 23.8 %collective-permute-start.6 = (bf16[5,128,1024]{2,1,0:T(8,128)(2,1)S(1)}, bf16[5,128,1024]{2,1,0:T(8,128)(2,1)}, u32[]{:S(2)}, u32[]{:S(2)}) collective-permute-start(bf16[5,128,1024]{2,1,0:T(8,128)(2,1)S(1)} %stack.6.refs_0_), channel_id=1, source_target_pairs={{0,8},{8,0},{16,24},{24,16},{32,40},{40,32},{48,56},{56,48},{64,72... | collective-permute-start | bytes 3932168 | tf_op jit(solution)/shard_map/ppermute | solution.py:37
  48.4 7.7 %collective-permute-start.8 = (bf16[128,1024]{1,0:T(8,128)(2,1)S(1)}, bf16[128,1024]{1,0:T(8,128)(2,1)S(1)}, u32[]{:S(2)}, u32[]{:S(2)}) collective-permute-start(bf16[128,1024]{1,0:T(8,128)(2,1)S(1)} %collective-permute-done.5.refs_4_), channel_id=1, source_target_pairs={{16,0},{24,8},{32,16},{40,24},{48,32},{56,40},{64,48},{72,56},{80,... | collective-permute-start | bytes 786440 | tf_op jit(solution)/shard_map/ppermute | solution.py:59
  48.4 9.3 %collective-permute-start.7 = (bf16[128,1024]{1,0:T(8,128)(2,1)S(1)}, bf16[128,1024]{1,0:T(8,128)(2,1)S(1)}, u32[]{:S(2)}, u32[]{:S(2)}) collective-permute-start(bf16[128,1024]{1,0:T(8,128)(2,1)S(1)} %collective-permute-done.4.refs_3_), channel_id=1, source_target_pairs={{0,16},{8,24},{16,32},{24,40},{32,48},{40,56},{48,64},{56,72},{64,... | collective-permute-start | bytes 786440 | tf_op jit(solution)/shard_map/ppermute | solution.py:58
  56.1 3.9 %collective-permute-start.11 = (bf16[64,1024]{1,0:T(8,128)(2,1)S(1)}, bf16[64,1024]{1,0:T(8,128)(2,1)S(1)}, u32[]{:S(2)}, u32[]{:S(2)}) collective-permute-start(bf16[64,1024]{1,0:T(8,128)(2,1)S(1)} %slice.65), channel_id=1, source_target_pairs={{16,0},{24,8},{32,16},{40,24},{48,32},{56,40},{64,48},{72,56},{80,... | collective-permute-start | bytes 393224 | tf_op jit(solution)/shard_map/ppermute | solution.py:59
  57.7 5.1 %collective-permute-start.10 = (bf16[64,1024]{1,0:T(8,128)(2,1)S(1)}, bf16[64,1024]{1,0:T(8,128)(2,1)S(1)}, u32[]{:S(2)}, u32[]{:S(2)}) collective-permute-start(bf16[64,1024]{1,0:T(8,128)(2,1)S(1)} %slice.64), channel_id=1, source_target_pairs={{0,16},{8,24},{16,32},{24,40},{32,48},{40,56},{48,64},{56,72},{64,... | collective-permute-start | bytes 393224 | tf_op jit(solution)/shard_map/ppermute | solution.py:58
  57.9 13.4 %collective-permute-start.9 = (bf16[2,128,1024]{2,1,0:T(8,128)(2,1)S(1)}, bf16[2,128,1024]{2,1,0:T(8,128)(2,1)}, u32[]{:S(2)}, u32[]{:S(2)}) collective-permute-start(bf16[2,128,1024]{2,1,0:T(8,128)(2,1)S(1)} %stack.7.refs_2_), channel_id=1, source_target_pairs={{0,8},{8,0},{16,24},{24,16},{32,40},{40,32},{48,56},{56,48},{64,72... | collective-permute-start | bytes 1572872 | tf_op jit(solution)/shard_map/ppermute | solution.py:37
  62.9 8.4 %collective-permute-start.12 = (bf16[2,64,1024]{2,1,0:T(8,128)(2,1)S(1)}, bf16[2,64,1024]{2,1,0:T(8,128)(2,1)S(1)}, u32[]{:S(2)}, u32[]{:S(2)}) collective-permute-start(bf16[2,64,1024]{2,1,0:T(8,128)(2,1)S(1)} %stack.8.refs_4_), channel_id=1, source_target_pairs={{0,8},{8,0},{16,24},{24,16},{32,40},{40,32},{48,56},{56,48},{64,72... | collective-permute-start | bytes 786440 | tf_op jit(solution)/shard_map/ppermute | solution.py:37
  67.6 1.6 copy-start
  69.3 1.7 copy-start.2
  71.3 4.4 %copy-start.11 = (bf16[2,128,256]{2,1,0:T(8,128)(2,1)S(1)}, bf16[2,128,256]{2,1,0:T(8,128)(2,1)}, u32[]{:S(2)}) copy-start(bf16[2,128,256]{2,1,0:T(8,128)(2,1)} %param.13) | copy-start | bytes 393220
  71.4 4.4 %copy-start.13 = (bf16[2,128,256]{2,1,0:T(8,128)(2,1)S(1)}, bf16[2,128,256]{2,1,0:T(8,128)(2,1)}, u32[]{:S(2)}) copy-start(bf16[2,128,256]{2,1,0:T(8,128)(2,1)} %param.12) | copy-start | bytes 393220
  73.5 7.7 %collective-permute-start.14 = (bf16[256,512]{1,0:T(8,128)(2,1)S(1)}, bf16[256,512]{1,0:T(8,128)(2,1)S(1)}, u32[]{:S(2)}, u32[]{:S(2)}) collective-permute-start(bf16[256,512]{1,0:T(8,128)(2,1)S(1)} %project.5.own_ref), channel_id=1, source_target_pairs={{8,16},{24,32},{40,48},{56,64},{72,80},{88,96},{104,112},{16,8},{3... | collective-permute-start | bytes 786440 | tf_op jit(solution)/shard_map/ppermute | solution.py:43
  75.4 5.8 %collective-permute-start.13 = (bf16[256,512]{1,0:T(8,128)(2,1)S(1)}, bf16[256,512]{1,0:T(8,128)(2,1)S(1)}, u32[]{:S(2)}, u32[]{:S(2)}) collective-permute-start(bf16[256,512]{1,0:T(8,128)(2,1)S(1)} %project.5.own_ref), channel_id=1, source_target_pairs={{0,8},{8,0},{16,24},{24,16},{32,40},{40,32},{48,56},{56,48},{64,72... | collective-permute-start | bytes 786440 | tf_op jit(solution)/shard_map/ppermute | solution.py:37
  75.8 2.0 copy-start.15
  75.8 2.0 copy-start.17
  75.8 5.4 %copy-start.3 = (f32[4,256,768]{2,1,0:T(8,128)S(1)}, f32[4,256,768]{2,1,0:T(8,128)}, u32[]{:S(2)}) copy-start(f32[4,256,768]{2,1,0:T(8,128)} %copy-done.2) | copy-start | bytes 9437188
  84.4 34.0 %all-to-all-start.1 = ((bf16[8,256,256]{2,1,0:T(8,128)(2,1)}), bf16[8,256,256]{2,1,0:T(8,128)(2,1)S(1)}, u32[]{:S(2)}, u32[]{:S(2)}) async-start(bf16[8,256,256]{2,1,0:T(8,128)(2,1)} %attend.2), calls=%async_computation.1 | async-start | bytes 2097152 | tf_op jit(solution)/shard_map/all_to_all | solution.py:32
  91.0 7.5 %collective-permute-start.17 = (bf16[128,1024]{1,0:T(8,128)(2,1)S(1)}, bf16[128,1024]{1,0:T(8,128)(2,1)S(1)}, u32[]{:S(2)}, u32[]{:S(2)}) collective-permute-start(bf16[128,1024]{1,0:T(8,128)(2,1)S(1)} %pad_maximum_fusion.refs_0_), channel_id=1, source_target_pairs={{16,0},{24,8},{32,16},{40,24},{48,32},{56,40},{64,48},{72,56},{80,... | collective-permute-start | bytes 786440 | tf_op jit(solution)/shard_map/ppermute | solution.py:59
  91.1 9.0 %collective-permute-start.15 = (bf16[128,1024]{1,0:T(8,128)(2,1)S(1)}, bf16[128,1024]{1,0:T(8,128)(2,1)S(1)}, u32[]{:S(2)}, u32[]{:S(2)}) collective-permute-start(bf16[128,1024]{1,0:T(8,128)(2,1)S(1)} %pad_maximum_fusion.refs_0_), channel_id=1, source_target_pairs={{0,16},{8,24},{16,32},{24,40},{32,48},{40,56},{48,64},{56,72},{64,... | collective-permute-start | bytes 786440 | tf_op jit(solution)/shard_map/ppermute | solution.py:58
  98.5 8.3 %collective-permute-start.18 = (bf16[128,1024]{1,0:T(8,128)(2,1)S(1)}, bf16[128,1024]{1,0:T(8,128)(2,1)S(1)}, u32[]{:S(2)}, u32[]{:S(2)}) collective-permute-start(bf16[128,1024]{1,0:T(8,128)(2,1)S(1)} %collective-permute-done.17.refs_2_), channel_id=1, source_target_pairs={{16,0},{24,8},{32,16},{40,24},{48,32},{56,40},{64,48},{72,56},{80,... | collective-permute-start | bytes 786440 | tf_op jit(solution)/shard_map/ppermute | solution.py:59
  100.0 20.0 %copy-start.4 = (bf16[128,1024]{1,0:T(8,128)(2,1)}, bf16[128,1024]{1,0:T(8,128)(2,1)S(1)}, u32[]{:S(2)}) copy-start(bf16[128,1024]{1,0:T(8,128)(2,1)S(1)} %collective-permute-done.15.refs_1_) | copy-start | bytes 786436
  100.0 7.8 %collective-permute-start.16 = (bf16[128,1024]{1,0:T(8,128)(2,1)S(1)}, bf16[128,1024]{1,0:T(8,128)(2,1)S(1)}, u32[]{:S(2)}, u32[]{:S(2)}) collective-permute-start(bf16[128,1024]{1,0:T(8,128)(2,1)S(1)} %collective-permute-done.15.refs_1_), channel_id=1, source_target_pairs={{0,16},{8,24},{16,32},{24,40},{32,48},{40,56},{48,64},{56,72},{64,... | collective-permute-start | bytes 786440 | tf_op jit(solution)/shard_map/ppermute | solution.py:58
  120.1 31.6 %all-to-all-start.2 = ((bf16[8,256,256]{2,1,0:T(8,128)(2,1)}), bf16[8,256,256]{2,1,0:T(8,128)(2,1)}, u32[]{:S(2)}, u32[]{:S(2)}) async-start(bf16[8,256,256]{2,1,0:T(8,128)(2,1)} %summed.1), calls=%async_computation.2 | async-start | bytes 2097152 | tf_op jit(solution)/shard_map/all_to_all | solution.py:32
  125.5 29.3 %collective-permute-start.19 = (bf16[5,128,1024]{2,1,0:T(8,128)(2,1)S(1)}, bf16[5,128,1024]{2,1,0:T(8,128)(2,1)}, u32[]{:S(2)}, u32[]{:S(2)}) collective-permute-start(bf16[5,128,1024]{2,1,0:T(8,128)(2,1)S(1)} %stack.9.refs_0_), channel_id=1, source_target_pairs={{0,8},{8,0},{16,24},{24,16},{32,40},{40,32},{48,56},{56,48},{64,72... | collective-permute-start | bytes 3932168 | tf_op jit(solution)/shard_map/ppermute | solution.py:37
  126.1 7.8 %collective-permute-start.21 = (bf16[128,1024]{1,0:T(8,128)(2,1)S(1)}, bf16[128,1024]{1,0:T(8,128)(2,1)S(1)}, u32[]{:S(2)}, u32[]{:S(2)}) collective-permute-start(bf16[128,1024]{1,0:T(8,128)(2,1)S(1)} %collective-permute-done.18.refs_4_), channel_id=1, source_target_pairs={{16,0},{24,8},{32,16},{40,24},{48,32},{56,40},{64,48},{72,56},{80,... | collective-permute-start | bytes 786440 | tf_op jit(solution)/shard_map/ppermute | solution.py:59
  126.1 8.9 %collective-permute-start.20 = (bf16[128,1024]{1,0:T(8,128)(2,1)S(1)}, bf16[128,1024]{1,0:T(8,128)(2,1)S(1)}, u32[]{:S(2)}, u32[]{:S(2)}) collective-permute-start(bf16[128,1024]{1,0:T(8,128)(2,1)S(1)} %collective-permute-done.16.refs_3_), channel_id=1, source_target_pairs={{0,16},{8,24},{16,32},{24,40},{32,48},{40,56},{48,64},{56,72},{64,... | collective-permute-start | bytes 786440 | tf_op jit(solution)/shard_map/ppermute | solution.py:58
  135.0 19.8 %collective-permute-start.22 = (bf16[2,128,1024]{2,1,0:T(8,128)(2,1)S(1)}, bf16[2,128,1024]{2,1,0:T(8,128)(2,1)}, u32[]{:S(2)}, u32[]{:S(2)}) collective-permute-start(bf16[2,128,1024]{2,1,0:T(8,128)(2,1)S(1)} %stack.10.refs_2_), channel_id=1, source_target_pairs={{0,8},{8,0},{16,24},{24,16},{32,40},{40,32},{48,56},{56,48},{64,72... | collective-permute-start | bytes 1572872 | tf_op jit(solution)/shard_map/ppermute | solution.py:37
  136.2 5.2 %collective-permute-start.24 = (bf16[64,1024]{1,0:T(8,128)(2,1)S(1)}, bf16[64,1024]{1,0:T(8,128)(2,1)S(1)}, u32[]{:S(2)}, u32[]{:S(2)}) collective-permute-start(bf16[64,1024]{1,0:T(8,128)(2,1)S(1)} %slice.67), channel_id=1, source_target_pairs={{16,0},{24,8},{32,16},{40,24},{48,32},{56,40},{64,48},{72,56},{80,... | collective-permute-start | bytes 393224 | tf_op jit(solution)/shard_map/ppermute | solution.py:59
  136.6 6.2 %collective-permute-start.23 = (bf16[64,1024]{1,0:T(8,128)(2,1)S(1)}, bf16[64,1024]{1,0:T(8,128)(2,1)S(1)}, u32[]{:S(2)}, u32[]{:S(2)}) collective-permute-start(bf16[64,1024]{1,0:T(8,128)(2,1)S(1)} %slice.66), channel_id=1, source_target_pairs={{0,16},{8,24},{16,32},{24,40},{32,48},{40,56},{48,64},{56,72},{64,... | collective-permute-start | bytes 393224 | tf_op jit(solution)/shard_map/ppermute | solution.py:58
  142.8 12.0 %collective-permute-start.25 = (bf16[2,64,1024]{2,1,0:T(8,128)(2,1)S(1)}, bf16[2,64,1024]{2,1,0:T(8,128)(2,1)S(1)}, u32[]{:S(2)}, u32[]{:S(2)}) collective-permute-start(bf16[2,64,1024]{2,1,0:T(8,128)(2,1)S(1)} %stack.11.refs_4_), channel_id=1, source_target_pairs={{0,8},{8,0},{16,24},{24,16},{32,40},{40,32},{48,56},{56,48},{64,72... | collective-permute-start | bytes 786440 | tf_op jit(solution)/shard_map/ppermute | solution.py:37
  156.9 9.6 %collective-permute-start.27 = (bf16[256,512]{1,0:T(8,128)(2,1)S(1)}, bf16[256,512]{1,0:T(8,128)(2,1)S(1)}, u32[]{:S(2)}, u32[]{:S(2)}) collective-permute-start(bf16[256,512]{1,0:T(8,128)(2,1)S(1)} %project.7.own_ref), channel_id=1, source_target_pairs={{8,16},{24,32},{40,48},{56,64},{72,80},{88,96},{104,112},{16,8},{3... | collective-permute-start | bytes 786440 | tf_op jit(solution)/shard_map/ppermute | solution.py:43
  162.4 4.0 %collective-permute-start.26 = (bf16[256,512]{1,0:T(8,128)(2,1)S(1)}, bf16[256,512]{1,0:T(8,128)(2,1)S(1)}, u32[]{:S(2)}, u32[]{:S(2)}) collective-permute-start(bf16[256,512]{1,0:T(8,128)(2,1)S(1)} %project.7.own_ref), channel_id=1, source_target_pairs={{0,8},{8,0},{16,24},{24,16},{32,40},{40,32},{48,56},{56,48},{64,72... | collective-permute-start | bytes 786440 | tf_op jit(solution)/shard_map/ppermute | solution.py:37
  162.6 3.9 %copy-start.1 = (f32[4,256,768]{2,1,0:T(8,128)S(1)}, f32[4,256,768]{2,1,0:T(8,128)}, u32[]{:S(2)}) copy-start(f32[4,256,768]{2,1,0:T(8,128)} %copy-done) | copy-start | bytes 9437188
  199.3 9.3 %copy-start.7 = (bf16[256,256]{1,0:T(8,128)(2,1)S(1)}, bf16[256,256]{1,0:T(8,128)(2,1)}, u32[]{:S(2)}) copy-start(bf16[256,256]{1,0:T(8,128)(2,1)} %copy-done.6) | copy-start | bytes 393220
  (3 other events, 2.5 us)
